TPU v7x, 32 devices: a whole 2x2x4 slice. The times are simulated.
32 devices in a mesh: sp: 8 (over z, x), tp: 4 (over y, core).
Axes of the slice: x: 2, y: 2, z: 4, core: 2. Of those that a mesh axis runs over, the one named last changes fastest.
Arguments:
- mid_state: bfloat16 [2048, 2048], P('sp'), may hold values from -6 to 6
- conv_pre: bfloat16 [2048, 1024], P('sp', 'tp'), may hold values from -8 to 8
- conv_taps: bfloat16 [31, 1024], P(None, 'tp'), may hold values from -1 to 1
- out_proj: bfloat16 [1024, 2048], P('tp'), may hold values from -0.1875 to 0.1875
- route_expert: int32 [2048, 2], P('sp'), may hold values from 0 to 7, as said below
- route_weight: float32 [2048, 2], P('sp'), may hold values from 0.1 to 1
- gate_w: bfloat16 [8, 2048, 2048], P('sp', None, 'tp'), may hold values from -0.125 to 0.125
- up_w: bfloat16 [8, 2048, 2048], P('sp', None, 'tp'), may hold values from -0.125 to 0.125
- down_w: bfloat16 [8, 2048, 2048], P('sp', 'tp'), may hold values from -0.125 to 0.125
- cotangent: bfloat16 [2048, 2048], P('sp'), may hold values from -6 to 6
Outputs:
- grad_gate: bfloat16 [8, 2048, 2048], P('sp', None, 'tp')
- grad_up: bfloat16 [8, 2048, 2048], P('sp', None, 'tp')
- grad_down: bfloat16 [8, 2048, 2048], P('sp', 'tp')
- grad_proj: float32 [2048, 1024], P('sp', 'tp')
- conv_input_grad: float32 [2048, 1024], P('sp', 'tp')
Inputs may be any that keep to these rules, and one draw needn't show every extreme that they name: `route_expert`: the two experts of a token are different and lie in one group of 8 // 4 consecutive experts; in every draw some expert is named by more than 68 routes of every aligned block of 256 tokens.
All inputs are finite; a program needn't handle non-finite values.
Results may differ from a plain program's by a relative error of at most 0.02.
Values may be sent and summed in bfloat16 or wider, within the bound.
A program may use at most 128 MiB of HBM per device.

v0:
```python
import jax
import jax.numpy as jnp
from jax import lax
from jax.experimental import pallas as pl
from jax.experimental.pallas import tpu as pltpu
from jax.sharding import PartitionSpec as P

D = 2048
KERNEL = 31
TOP = 2
GROUPS = 4
MESH = pl.DeviceIdType.MESH


def passed_along(value, axis, steps):
    count = lax.axis_size(axis)
    initial, last = (max(0, -steps), min(count, count - steps))
    return lax.ppermute(value, axis, [(source, source + steps) for source in range(initial, last)])


def silu_slope(value):
    sig = jax.nn.sigmoid(value)
    return sig * (1.0 + value * (1.0 - sig))


def body(
    mid_state,
    conv_pre,
    conv_taps,
    out_proj,
    route_expert,
    route_weight,
    gate_w,
    up_w,
    down_w,
    cotangent,
):
    groups = lax.axis_size("sp")
    token_count = mid_state.shape[0]
    slot_count = 17 * token_count * TOP // (16 * groups)
    flat_routes = route_expert.reshape(-1)
    one_hot_table = (flat_routes[:, None] == jnp.arange(groups, dtype=jnp.int32)[None, :]).astype(
        jnp.int32
    )
    slot_rank = jnp.sum(jnp.cumsum(one_hot_table, axis=0) * one_hot_table, axis=1) - 1
    kept_mask = slot_rank < slot_count
    slot_index = jnp.where(kept_mask, flat_routes * slot_count + slot_rank, groups * slot_count)
    token_ids = jnp.arange(token_count * TOP, dtype=jnp.int32) // TOP
    route_cot = (
        route_weight.reshape(-1)[:, None] * cotangent[token_ids].astype(jnp.float32)
    ).astype(jnp.bfloat16)
    send_inputs = (
        jnp.zeros((groups * slot_count, D), jnp.bfloat16)
        .at[slot_index]
        .set(mid_state[token_ids], mode="drop")
        .reshape(groups, slot_count, D)
    )
    send_seeds = (
        jnp.zeros((groups * slot_count, D), jnp.bfloat16)
        .at[slot_index]
        .set(route_cot, mode="drop")
        .reshape(groups, slot_count, D)
    )
    got_inputs, got_seeds = (
        lax.all_to_all(send_inputs, "sp", split_axis=0, concat_axis=0, tiled=True),
        lax.all_to_all(send_seeds, "sp", split_axis=0, concat_axis=0, tiled=True),
    )
    inputs = got_inputs.reshape(groups * slot_count, D)
    seeds = got_seeds.reshape(groups * slot_count, D)
    gate_mat = gate_w[0]
    up_mat = up_w[0]
    down_mat = down_w[0]
    gate_pre = jnp.dot(inputs, gate_mat, preferred_element_type=jnp.float32)
    up_pre = jnp.dot(inputs, up_mat, preferred_element_type=jnp.float32)
    gate_act = jax.nn.silu(gate_pre)
    hidden = (gate_act * up_pre).astype(jnp.bfloat16)
    hidden_grad = lax.dot_general(
        seeds, down_mat, (((1,), (1,)), ((), ())), preferred_element_type=jnp.float32
    )
    gate_grad = (hidden_grad * up_pre * silu_slope(gate_pre)).astype(jnp.bfloat16)
    up_grad = (hidden_grad * gate_act).astype(jnp.bfloat16)
    grad_down = lax.dot_general(
        hidden, seeds, (((0,), (0,)), ((), ())), preferred_element_type=jnp.float32
    ).astype(jnp.bfloat16)
    grad_gate = lax.dot_general(
        inputs, gate_grad, (((0,), (0,)), ((), ())), preferred_element_type=jnp.float32
    ).astype(jnp.bfloat16)
    grad_up = lax.dot_general(
        inputs, up_grad, (((0,), (0,)), ((), ())), preferred_element_type=jnp.float32
    ).astype(jnp.bfloat16)
    weight_results = (grad_gate, grad_up, grad_down)
    partial_value = lax.dot_general(
        gate_grad, gate_mat, (((1,), (1,)), ((), ())), preferred_element_type=jnp.float32
    )
    partial_value = partial_value + lax.dot_general(
        up_grad, up_mat, (((1,), (1,)), ((), ())), preferred_element_type=jnp.float32
    )
    partial_value = partial_value.astype(jnp.bfloat16).astype(jnp.float32)
    safe_index = jnp.minimum(slot_index, groups * slot_count - 1)
    slice_width = D // lax.axis_size("tp")
    summed = lax.psum_scatter(
        partial_value.astype(jnp.bfloat16), "tp", scatter_dimension=1, tiled=True
    )
    returned = lax.all_to_all(
        summed.reshape(groups, slot_count, slice_width),
        "sp",
        split_axis=0,
        concat_axis=0,
        tiled=True,
    ).reshape(groups * slot_count, slice_width)
    picked = jnp.where(
        kept_mask[:, None], returned[safe_index].astype(jnp.float32), jnp.float32(0.0)
    )
    moe_grad = jnp.sum(picked.reshape(token_count, TOP, slice_width), axis=1)
    own_cot = lax.dynamic_slice_in_dim(
        cotangent, lax.axis_index("tp") * slice_width, slice_width, 1
    )
    mid_part = (own_cot.astype(jnp.float32) + moe_grad).astype(jnp.bfloat16)
    mid_grad = lax.all_gather(mid_part, "tp", axis=1, tiled=True)
    grad_gate, grad_up, grad_down = weight_results
    pre_float = conv_pre.astype(jnp.float32)
    activated = jax.nn.silu(pre_float).astype(jnp.bfloat16)
    mixed_grad = lax.dot_general(
        mid_grad, out_proj, (((1,), (1,)), ((), ())), preferred_element_type=jnp.float32
    )
    conv_grad = (mixed_grad * silu_slope(pre_float)).astype(jnp.bfloat16)
    next_head = passed_along(conv_grad[: KERNEL - 1], "sp", -1)
    extended = jnp.concatenate([conv_grad, next_head], axis=0).astype(jnp.float32)
    conv_input_grad = jnp.zeros(conv_grad.shape, jnp.float32)
    for lag_index in range(KERNEL):
        conv_input_grad = (
            conv_input_grad
            + conv_taps[lag_index].astype(jnp.float32)[None, :]
            * extended[lag_index : lag_index + token_count]
        )
    grad_proj = lax.psum_scatter(
        lax.dot_general(
            mid_grad, activated, (((0,), (0,)), ((), ())), preferred_element_type=jnp.float32
        ).astype(jnp.bfloat16),
        "sp",
        scatter_dimension=0,
        tiled=True,
    ).astype(jnp.float32)
    return (grad_gate[None], grad_up[None], grad_down[None], grad_proj, conv_input_grad)


def dispatch_kernel(send_m, send_c, send_w, out_m, out_c, out_w, s_sem, r_sem, w_sem, l_sem):
    sp, tp = lax.axis_index("sp"), lax.axis_index("tp")
    planes, slots, width = send_m.shape
    plane, side = sp // TOP, sp % TOP
    row, core = tp // 2, tp % 2
    across = (TOP * plane + 1 - side, tp)
    along = (sp, 2 * (1 - row) + core)
    partner = (sp, 2 * row + 1 - core)

    barrier = pltpu.get_barrier_semaphore()
    targets = [across, along, partner]
    targets += [(TOP * ((plane + k) % planes) + side, tp) for k in range(1, planes)]
    for target in targets:
        pl.semaphore_signal(barrier, inc=1, device_id=target, device_id_type=MESH)
    pl.semaphore_wait(barrier, len(targets))

    sends = (send_m, send_c)
    outs = (out_m, out_c)

    def place(array, block, quarter):
        return outs[array].at[block, :, pl.ds(pl.multiple_of(quarter * width, width), width)]

    def remote(source, target_ref, kind, k, array, device):
        return pltpu.make_async_remote_copy(
            src_ref=source,
            dst_ref=target_ref,
            send_sem=s_sem.at[kind, k, array],
            recv_sem=r_sem.at[kind, k, array],
            device_id=device,
            device_id_type=MESH,
        )

    def weights(source, block, kind, k, device):
        return pltpu.make_async_remote_copy(
            src_ref=source,
            dst_ref=out_w.at[block],
            send_sem=w_sem.at[0, kind, k],
            recv_sem=w_sem.at[1, kind, k],
            device_id=device,
            device_id_type=MESH,
        )

    copies = []
    arrivals = {}
    own = TOP * plane + side
    for k in range(1, planes):
        to = (plane - k + planes) % planes
        device = (TOP * to + side, tp)
        for array in range(2):
            copy = remote(sends[array].at[to], place(array, own, tp), 0, k, array, device)
            copy.start()
            copies.append(copy)
            arrivals[0, k, array] = copy
        copy = weights(send_w.at[to], own, 0, k, device)
        copy.start()
        copies.append(copy)
        arrivals[0, k, 2] = copy

    local = []
    for array in range(2):
        local.append(pltpu.make_async_copy(sends[array].at[plane], place(array, own, tp), l_sem.at[array]))
    local.append(pltpu.make_async_copy(send_w.at[plane], out_w.at[own], l_sem.at[2]))
    for copy in local:
        copy.start()

    def forward(kind, k, array, block, quarter, device, source=None):
        ref = place(array, block, quarter)
        copy = remote(ref if source is None else source, ref, kind, k, array, device)
        copy.start()
        copies.append(copy)
        arrivals[kind, k, array] = copy

    other = 2 * (1 - row) + core
    for step in range(planes + 2):
        k = step
        if k < planes:
            block = TOP * ((plane + k) % planes) + side
            for array in range(2):
                if k > 0:
                    arrivals[0, k, array].wait_recv()
                source = sends[array].at[plane] if k == 0 else None
                forward(1, k, array, block, tp, across, source)
                forward(2, k, array, block, tp, along, source)
                forward(3, k, array, block, tp, partner, source)
            if k > 0:
                arrivals[0, k, 2].wait_recv()
            source = send_w.at[plane] if k == 0 else out_w.at[block]
            copy = weights(source, block, 1, k, across)
            copy.start()
            copies.append(copy)
            arrivals[1, k, 2] = copy
        k = step - 1
        if 0 <= k < planes:
            mine = TOP * ((plane + k) % planes) + side
            theirs = TOP * ((plane + k) % planes) + 1 - side
            arrivals[1, k, 0].wait_recv()
            forward(4, k, 0, theirs, tp, along)
            forward(5, k, 0, theirs, tp, partner)
            arrivals[2, k, 1].wait_recv()
            forward(4, k, 1, mine, other, across)
            forward(6, k, 1, mine, other, partner)
            arrivals[1, k, 1].wait_recv()
            forward(5, k, 1, theirs, tp, partner)
            arrivals[2, k, 0].wait_recv()
            forward(6, k, 0, mine, other, partner)
            arrivals[1, k, 2].wait_recv()
        k = step - 2
        if 0 <= k < planes:
            theirs = TOP * ((plane + k) % planes) + 1 - side
            for array in range(2):
                arrivals[4, k, array].wait_recv()
                forward(7, k, array, theirs, other, partner)
    for k in range(planes):
        for array in range(2):
            for kind in (3, 5, 6, 7):
                arrivals[kind, k, array].wait_recv()
    for copy in copies:
        copy.wait_send()
    for copy in local:
        copy.wait()


def dispatch(send_m, send_c, send_w):
    planes, slots, width = send_m.shape
    blocks = lax.axis_size("sp")
    vmem = pl.BlockSpec(memory_space=pltpu.VMEM)
    rows = jax.ShapeDtypeStruct((blocks, slots, width * lax.axis_size("tp")), send_m.dtype)
    return pl.pallas_call(
        dispatch_kernel,
        out_shape=(rows, rows, jax.ShapeDtypeStruct((blocks,) + send_w.shape[1:], send_w.dtype)),
        in_specs=[vmem] * 3,
        out_specs=(vmem, vmem, vmem),
        scratch_shapes=[
            pltpu.SemaphoreType.DMA((8, planes, 2)),
            pltpu.SemaphoreType.DMA((8, planes, 2)),
            pltpu.SemaphoreType.DMA((2, 2, planes)),
            pltpu.SemaphoreType.DMA((3,)),
        ],
        compiler_params=pltpu.CompilerParams(
            collective_id=0, has_side_effects=True, vmem_limit_bytes=32 * 1024 * 1024
        ),
        name="dispatch",
    )(send_m, send_c, send_w)


def dot(left, right, left_dim, right_dim):
    return lax.dot_general(
        left, right, (((left_dim,), (right_dim,)), ((), ())), preferred_element_type=jnp.float32
    )


def paired_body(
    mid_state,
    conv_pre,
    conv_taps,
    out_proj,
    route_expert,
    route_weight,
    gate_w,
    up_w,
    down_w,
    cotangent,
):
    experts = lax.axis_size("sp")
    tp_count = lax.axis_size("tp")
    token_count = mid_state.shape[0]
    slot_count = 17 * token_count * TOP // (16 * experts)
    slots = (slot_count + 7) // 8 * 8
    width = D // tp_count
    tp = lax.axis_index("tp")

    group = route_expert[:, 0] // TOP
    in_group = group[None, :] == jnp.arange(GROUPS, dtype=jnp.int32)[:, None]
    positions = jnp.arange(token_count, dtype=jnp.int32)
    earlier = (positions[:, None] < positions[None, :]).astype(jnp.bfloat16)
    ranks = dot(in_group.astype(jnp.bfloat16), earlier, 1, 0)
    rank = jnp.sum(jnp.where(in_group, ranks, 0.0), axis=0).astype(jnp.int32)
    slot = jnp.where(rank < slot_count, group * slots + rank, -1)
    taken = slot[None, :] == jnp.arange(GROUPS * slots, dtype=jnp.int32)[:, None]
    pick = taken.astype(jnp.bfloat16)
    own_state = lax.dynamic_slice_in_dim(mid_state, tp * width, width, 1)
    own_cot = lax.dynamic_slice_in_dim(cotangent, tp * width, width, 1)
    send_m = dot(pick, own_state, 1, 0).astype(jnp.bfloat16).reshape(GROUPS, slots, width)
    send_c = dot(pick, own_cot, 1, 0).astype(jnp.bfloat16).reshape(GROUPS, slots, width)
    swapped = (route_expert[:, 0] % TOP) != 0
    first = jnp.where(swapped, route_weight[:, 1], route_weight[:, 0])
    second = jnp.where(swapped, route_weight[:, 0], route_weight[:, 1])
    slot_weights = [
        jnp.sum(jnp.where(taken, each[None, :], 0.0), axis=1).reshape(GROUPS, 1, slots)
        for each in (first, second)
    ]
    send_w = jnp.pad(
        jnp.concatenate(slot_weights, axis=1), ((0, 0), (0, 8 - TOP), (0, -slots % 128))
    )
    got_m, got_c, got_w = dispatch(send_m, send_c, send_w)
    inputs = got_m.reshape(experts * slots, D)
    side = lax.axis_index("sp") % TOP
    weight = lax.dynamic_index_in_dim(got_w, side, 1, keepdims=False)[:, :slots]
    seeds = (
        (weight[:, :, None] * got_c.astype(jnp.float32))
        .astype(jnp.bfloat16)
        .reshape(experts * slots, D)
    )
    gate_mat = gate_w[0]
    up_mat = up_w[0]
    down_mat = down_w[0]
    gate_pre = dot(inputs, gate_mat, 1, 0)
    up_pre = dot(inputs, up_mat, 1, 0)
    gate_act = jax.nn.silu(gate_pre)
    hidden = (gate_act * up_pre).astype(jnp.bfloat16)
    hidden_grad = dot(seeds, down_mat, 1, 1)
    gate_grad = (hidden_grad * up_pre * silu_slope(gate_pre)).astype(jnp.bfloat16)
    up_grad = (hidden_grad * gate_act).astype(jnp.bfloat16)
    partial_value = (dot(gate_grad, gate_mat, 1, 1) + dot(up_grad, up_mat, 1, 1)).astype(
        jnp.bfloat16
    )
    summed = lax.psum_scatter(partial_value, "tp", scatter_dimension=1, tiled=True)
    returned = lax.all_to_all(
        summed.reshape(experts, slots, width), "sp", split_axis=0, concat_axis=0, tiled=True
    )
    pick_each = jnp.repeat(pick.reshape(GROUPS, 1, slots, token_count), TOP, axis=1)
    moe_grad = dot(
        pick_each.reshape(experts * slots, token_count),
        returned.reshape(experts * slots, width),
        0,
        0,
    )
    mid_part = (own_cot.astype(jnp.float32) + moe_grad).astype(jnp.bfloat16)
    mid_grad = lax.all_gather(mid_part, "tp", axis=1, tiled=True)
    grad_down = dot(hidden, seeds, 0, 0).astype(jnp.bfloat16)
    grad_gate = dot(inputs, gate_grad, 0, 0).astype(jnp.bfloat16)
    grad_up = dot(inputs, up_grad, 0, 0).astype(jnp.bfloat16)
    pre_float = conv_pre.astype(jnp.float32)
    activated = jax.nn.silu(pre_float).astype(jnp.bfloat16)
    mixed_grad = dot(mid_grad, out_proj, 1, 1)
    conv_grad = (mixed_grad * silu_slope(pre_float)).astype(jnp.bfloat16)
    next_head = passed_along(conv_grad[: KERNEL - 1], "sp", -1)
    extended = jnp.concatenate([conv_grad, next_head], axis=0).astype(jnp.float32)
    conv_input_grad = jnp.zeros(conv_grad.shape, jnp.float32)
    for lag_index in range(KERNEL):
        conv_input_grad = (
            conv_input_grad
            + conv_taps[lag_index].astype(jnp.float32)[None, :]
            * extended[lag_index : lag_index + token_count]
        )
    grad_proj = lax.psum_scatter(
        dot(mid_grad, activated, 0, 0).astype(jnp.bfloat16),
        "sp",
        scatter_dimension=0,
        tiled=True,
    ).astype(jnp.float32)
    return (grad_gate[None], grad_up[None], grad_down[None], grad_proj, conv_input_grad)


def solution(mesh):
    placed = (
        P("sp", None),
        P("sp", "tp"),
        P(None, "tp"),
        P("tp", None),
        P("sp", None),
        P("sp", None),
        P("sp", None, "tp"),
        P("sp", None, "tp"),
        P("sp", "tp", None),
        P("sp", None),
    )
    experts = mesh.shape["sp"]
    paired = experts == GROUPS * TOP and mesh.shape["tp"] == 4
    return jax.shard_map(
        paired_body if paired else body,
        mesh=mesh,
        in_specs=placed,
        out_specs=(
            P("sp", None, "tp"),
            P("sp", None, "tp"),
            P("sp", "tp", None),
            P("sp", "tp"),
            P("sp", "tp"),
        ),
        check_vma=False,
    )
```

profile of v0, /device:TPU:0, one launch (start us, length us, event | category | flops | bytes accessed | tf_op | source)
XLA Modules:
  0.0 205.6 jit_solution(2243185497464621221)
XLA Ops:
  7.2 0.0 copy-start
  7.2 0.0 reduce-scatter.3.cloned.1.call-start
  7.2 0.8 slice.204
  8.1 0.2 fusion.15
  8.3 1.2 convolution_convert_fusion.5
  9.5 1.2 convolution_convert_fusion.4
  10.7 0.8 fusion.67
  11.4 0.2 select_reduce_fusion.1
  11.6 0.1 reshape.146
  11.7 0.1 reshape.145
  11.8 35.1 %dispatch.1 = (bf16[8,72,2048]{2,1,0:T(8,128)(2,1)S(1)}, bf16[8,72,2048]{2,1,0:T(8,128)(2,1)S(1)}, f32[8,8,128]{2,1,0:T(8,128)S(1)}) custom-call(bf16[4,72,512]{2,1,0:T(8,128)(2,1)S(1)} %bitcast.79, bf16[4,72,512]{2,1,0:T(8,128)(2,1)S(1)} %bitcast.80, f32[4,8,128]{2,1,0:T(8,128)S(1)} %select_maximum_fusion.send_w), custom_call_target="tpu_custom_call" | custom-call | tf_op jit(solution)/shard_map/dispatch/pallas_call | solution.py:274
  47.0 0.0 copy-start.5
  47.0 2.4 %fusion.5 = f32[576,512]{1,0:T(8,128)} fusion(bf16[576,2048]{1,0:T(8,128)(2,1)S(1)} %bitcast.81, bf16[1,2048,512]{2,1,0:T(8,128)(2,1)S(1)} %copy-done), kind=kOutput, calls=%fused_computation.11 | convolution fusion | flops 1207959552 | bytes 5636096 | tf_op jit(solution)/shard_map/dot_general | solution.py:293
  49.4 0.3 copy-done.2
  49.7 0.5 copy-done.5
  50.1 2.5 %fusion.8 = f32[576,512]{1,0:T(8,128)} fusion(bf16[576,2048]{1,0:T(8,128)(2,1)S(1)} %bitcast.82, bf16[1,2048,512]{2,1,0:T(8,128)(2,1)S(1)} %copy-done.5), kind=kOutput, calls=%fused_computation.14 | convolution fusion | flops 1207959552 | bytes 5636096 | tf_op jit(solution)/shard_map/dot_general | solution.py:293
  52.6 0.0 copy-start.12
  52.6 2.3 %multiply_convert_fusion = bf16[8,72,2048]{2,1,0:T(8,128)(2,1)S(1)} fusion(bf16[8,72,2048]{2,1,0:T(8,128)(2,1)} %copy-done.1, f32[8,72]{1,0:T(8,128)S(1)} %bitcast.92), kind=kLoop, calls=%fused_computation.1 | loop fusion | flops 3538944 | bytes 4720896 | tf_op jit(solution)/shard_map/convert_element_type | solution.py:347
  54.9 0.3 copy-done.12
  55.2 0.4 copy-done.14
  55.6 1.8 multiply_convert_fusion.2
  57.3 0.0 copy-start.6
  57.4 1.4 fusion.3
  58.8 0.2 copy-done.6
  58.9 2.9 %add_convert_fusion = bf16[576,2048]{1,0:T(8,128)(2,1)} fusion(f32[576,2048]{1,0:T(8,128)S(1)} %fusion.3, bf16[576,512]{1,0:T(8,128)(2,1)S(1)} %get-tuple-element.13, bf16[1,2048,512]{2,1,0:T(8,128)(2,1)S(1)} %copy-done.6), kind=kOutput, calls=%fused_computation | convolution fusion | flops 1210318848 | bytes 9764864 | tf_op jit(solution)/shard_map/dot_general | solution.py:293
  61.8 0.0 reduce-scatter.3.cloned.1.call-update
  61.8 29.4 %reduce-scatter.3.cloned.1.call-done = bf16[576,512]{1,0:T(8,128)(2,1)} async-done(((bf16[576,2048]{1,0:T(8,128)(2,1)}), bf16[576,512]{1,0:T(8,128)(2,1)}) %reduce-scatter.3.cloned.1.call-update) | async-done | bytes 589840 | tf_op jit(solution)/shard_map/reduce_scatter | solution.py:363
  91.2 5.5 %all-to-all-start = ((bf16[8,72,512]{2,1,0:T(8,128)(2,1)}), bf16[8,72,512]{2,1,0:T(8,128)(2,1)}, u32[]{:S(2)}, u32[]{:S(2)}) async-start(bf16[8,72,512]{2,1,0:T(8,128)(2,1)} %bitcast.87), calls=%async_computation.1 | async-start | bytes 1179648 | tf_op jit(solution)/shard_map/all_to_all | solution.py:364
  96.7 0.0 all-gather.2.cloned.1.call-start
  96.8 0.1 compare_convert_fusion
  96.9 15.6 %all-to-all-done = bf16[8,72,512]{2,1,0:T(8,128)(2,1)} async-done(((bf16[8,72,512]{2,1,0:T(8,128)(2,1)}), bf16[8,72,512]{2,1,0:T(8,128)(2,1)}, u32[]{:S(2)}, u32[]{:S(2)}) %all-to-all-start) | async-done | bytes 589856 | tf_op jit(solution)/shard_map/all_to_all | solution.py:364
  112.5 2.2 %fusion.12 = bf16[256,512]{1,0:T(8,128)(2,1)} fusion(bf16[576,256]{1,0:T(8,128)(2,1)S(1)} %bitcast.88, bf16[576,512]{1,0:T(8,128)(2,1)} %bitcast.16, bf16[256,2048]{1,0:T(8,128)(2,1)} %param.19, s32[]{:T(128)S(6)} %select_n.77), kind=kOutput, calls=%fused_computation.21 | convolution fusion | flops 151388160 | bytes 1409028 | tf_op jit(solution)/shard_map/dot_general | solution.py:293
  114.8 0.0 all-gather.2.cloned.1.call-update
  114.8 0.0 copy-start.11
  114.8 0.2 reduce-scatter.5.cloned.1.call-start
  115.0 4.8 %fusion = bf16[1,2048,512]{2,1,0:T(8,128)(2,1)} fusion(bf16[576,2048]{1,0:T(8,128)(2,1)} %bitcast.83, bf16[576,512]{1,0:T(8,128)(2,1)S(1)} %get-tuple-element.14), kind=kOutput, calls=%fused_computation.5 | convolution fusion | flops 1209008128 | bytes 5046272 | tf_op jit(solution)/shard_map/dot_general | solution.py:293
  119.9 9.9 %all-gather.2.cloned.1.call-done = bf16[256,2048]{1,0:T(8,128)(2,1)} async-done(((bf16[256,512]{1,0:T(8,128)(2,1)}), bf16[256,2048]{1,0:T(8,128)(2,1)}) %all-gather.2.cloned.1.call-update) | async-done | bytes 1048592 | tf_op jit(solution)/shard_map/all_gather | solution.py:375
  129.8 2.7 %convolution_convert_fusion.3 = bf16[2048,256]{1,0:T(8,128)(2,1)} fusion(bf16[256,2048]{1,0:T(8,128)(2,1)} %all-gather.2.cloned.1.call-done, bf16[256,256]{1,0:T(8,128)(2,1)S(1)} %copy-done.11), kind=kOutput, calls=%fused_computation.8 | convolution fusion | flops 269352960 | bytes 2228224 | tf_op jit(solution)/shard_map/dot_general | solution.py:293
  132.5 0.0 reduce-scatter.5.cloned.1.call-update
  132.6 5.0 %fusion.1 = bf16[1,2048,512]{2,1,0:T(8,128)(2,1)} fusion(bf16[576,2048]{1,0:T(8,128)(2,1)} %bitcast.84, bf16[576,512]{1,0:T(8,128)(2,1)S(1)} %get-tuple-element.13), kind=kOutput, calls=%fused_computation.6 | convolution fusion | flops 1209008128 | bytes 5046272 | tf_op jit(solution)/shard_map/dot_general | solution.py:293
  137.6 0.0 copy-start.9
  137.6 3.3 %fusion.2 = bf16[1,512,2048]{2,1,0:T(8,128)(2,1)} fusion(bf16[576,2048]{1,0:T(8,128)(2,1)S(1)} %bitcast.86, f32[576,512]{1,0:T(8,128)S(1)} %copy-done.15, f32[576,512]{1,0:T(8,128)S(1)} %copy-done.13), kind=kOutput, calls=%fused_computation.7 | convolution fusion | flops 1210777600 | bytes 6815744 | tf_op jit(solution)/shard_map/dot_general | solution.py:293
  140.9 0.5 fusion.14
  141.4 1.3 collective-permute-start
  142.7 4.3 %collective-permute-done = bf16[30,256]{1,0:T(8,128)(2,1)S(1)} collective-permute-done((bf16[30,256]{1,0:T(8,128)(2,1)S(1)}, bf16[30,256]{1,0:T(8,128)(2,1)S(1)}, u32[]{:S(2)}, u32[]{:S(2)}) %collective-permute-start) | collective-permute-done | bytes 15392 | tf_op jit(solution)/shard_map/ppermute | solution.py:18
  147.1 1.4 fusion.22
  148.5 49.0 %reduce-scatter.5.cloned.1.call-done = bf16[256,256]{1,0:T(8,128)(2,1)} async-done(((bf16[2048,256]{1,0:T(8,128)(2,1)}), bf16[256,256]{1,0:T(8,128)(2,1)}) %reduce-scatter.5.cloned.1.call-update) | async-done | bytes 131088 | tf_op jit(solution)/shard_map/reduce_scatter | solution.py:392
  197.4 1.6 convert_element_type.153
  (32 shorter events, 0.2 us)
Async XLA Ops:
  7.2 39.8 %copy-start = (bf16[1,2048,512]{2,1,0:T(8,128)(2,1)S(1)}, bf16[1,2048,512]{2,1,0:T(8,128)(2,1)}, u32[]{:S(2)}) copy-start(bf16[1,2048,512]{2,1,0:T(8,128)(2,1)} %param.16) | copy-start | bytes 6291460
  7.2 84.0 %reduce-scatter.3.cloned.1.call-start = ((), (), s32[]{:S(2)}) async-start(), calls=%async_computation.3 | async-start | bytes 2949120 | tf_op jit(solution)/shard_map/reduce_scatter | solution.py:363
  47.0 2.4 %copy-start.1 = (bf16[8,72,2048]{2,1,0:T(8,128)(2,1)}, bf16[8,72,2048]{2,1,0:T(8,128)(2,1)S(1)}, u32[]{:S(2)}) copy-start(bf16[8,72,2048]{2,1,0:T(8,128)(2,1)S(1)} %get-tuple-element.10) | copy-start | bytes 7077892
  47.0 2.7 %copy-start.2 = (bf16[8,72,2048]{2,1,0:T(8,128)(2,1)}, bf16[8,72,2048]{2,1,0:T(8,128)(2,1)S(1)}, u32[]{:S(2)}) copy-start(bf16[8,72,2048]{2,1,0:T(8,128)(2,1)S(1)} %get-tuple-element.8) | copy-start | bytes 7077892
  47.0 3.1 %copy-start.5 = (bf16[1,2048,512]{2,1,0:T(8,128)(2,1)S(1)}, bf16[1,2048,512]{2,1,0:T(8,128)(2,1)}, u32[]{:S(2)}) copy-start(bf16[1,2048,512]{2,1,0:T(8,128)(2,1)} %param.17) | copy-start | bytes 6291460
  52.6 2.3 %copy-start.8 = (bf16[1,512,2048]{2,1,0:T(8,128)(2,1)S(1)}, bf16[1,512,2048]{2,1,0:T(8,128)(2,1)}, u32[]{:S(2)}) copy-start(bf16[1,512,2048]{2,1,0:T(8,128)(2,1)} %param.18) | copy-start | bytes 6291460
  52.6 2.6 %copy-start.12 = (f32[576,512]{1,0:T(8,128)S(1)}, f32[576,512]{1,0:T(8,128)}, u32[]{:S(2)}) copy-start(f32[576,512]{1,0:T(8,128)} %fusion.5) | copy-start | bytes 3538948
  52.6 2.9 %copy-start.14 = (f32[576,512]{1,0:T(8,128)S(1)}, f32[576,512]{1,0:T(8,128)}, u32[]{:S(2)}) copy-start(f32[576,512]{1,0:T(8,128)} %fusion.8) | copy-start | bytes 3538948
  54.9 2.4 %copy-start.3 = (bf16[8,72,2048]{2,1,0:T(8,128)(2,1)}, bf16[8,72,2048]{2,1,0:T(8,128)(2,1)S(1)}, u32[]{:S(2)}) copy-start(bf16[8,72,2048]{2,1,0:T(8,128)(2,1)S(1)} %multiply_convert_fusion) | copy-start | bytes 7077892
  57.3 1.6 copy-start.6
  91.2 21.3 %all-to-all-start = ((bf16[8,72,512]{2,1,0:T(8,128)(2,1)}), bf16[8,72,512]{2,1,0:T(8,128)(2,1)}, u32[]{:S(2)}, u32[]{:S(2)}) async-start(bf16[8,72,512]{2,1,0:T(8,128)(2,1)} %bitcast.87), calls=%async_computation.1 | async-start | bytes 1179648 | tf_op jit(solution)/shard_map/all_to_all | solution.py:364
  96.7 33.1 %all-gather.2.cloned.1.call-start = ((), (), s32[]{:S(2)}) async-start(), calls=%async_computation.4 | async-start | bytes 1310720 | tf_op jit(solution)/shard_map/all_gather | solution.py:375
  114.8 15.0 %copy-start.11 = (bf16[256,256]{1,0:T(8,128)(2,1)S(1)}, bf16[256,256]{1,0:T(8,128)(2,1)}, u32[]{:S(2)}) copy-start(bf16[256,256]{1,0:T(8,128)(2,1)} %param.11) | copy-start | bytes 393220
  114.8 82.6 %reduce-scatter.5.cloned.1.call-start = ((), (), s32[]{:S(2)}) async-start(), calls=%async_computation.5 | async-start | bytes 1179648 | tf_op jit(solution)/shard_map/reduce_scatter | solution.py:392
  119.9 12.7 %copy-start.7 = (bf16[31,256]{1,0:T(8,128)(2,1)S(1)}, bf16[31,256]{1,0:T(8,128)(2,1)}, u32[]{:S(2)}) copy-start(bf16[31,256]{1,0:T(8,128)(2,1)} %param.12) | copy-start | bytes 47620
  132.6 5.0 %copy-start.4 = (bf16[8,72,2048]{2,1,0:T(8,128)(2,1)S(1)}, bf16[8,72,2048]{2,1,0:T(8,128)(2,1)}, u32[]{:S(2)}) copy-start(bf16[8,72,2048]{2,1,0:T(8,128)(2,1)} %copy-done.3) | copy-start | bytes 7077892
  132.6 5.0 %copy-start.13 = (f32[576,512]{1,0:T(8,128)S(1)}, f32[576,512]{1,0:T(8,128)}, u32[]{:S(2)}) copy-start(f32[576,512]{1,0:T(8,128)} %fusion.5) | copy-start | bytes 3538948
  132.6 5.0 %copy-start.15 = (f32[576,512]{1,0:T(8,128)S(1)}, f32[576,512]{1,0:T(8,128)}, u32[]{:S(2)}) copy-start(f32[576,512]{1,0:T(8,128)} %fusion.8) | copy-start | bytes 3538948
  137.6 3.3 %copy-start.9 = (bf16[256,2048]{1,0:T(8,128)(2,1)S(1)}, bf16[256,2048]{1,0:T(8,128)(2,1)}, u32[]{:S(2)}) copy-start(bf16[256,2048]{1,0:T(8,128)(2,1)} %param.13) | copy-start | bytes 3145732
  137.6 3.3 %copy-start.10 = (bf16[256,2048]{1,0:T(8,128)(2,1)S(1)}, bf16[256,2048]{1,0:T(8,128)(2,1)}, u32[]{:S(2)}) copy-start(bf16[256,2048]{1,0:T(8,128)(2,1)} %all-gather.2.cloned.1.call-done) | copy-start | bytes 3145732
  141.4 5.6 %collective-permute-start = (bf16[30,256]{1,0:T(8,128)(2,1)S(1)}, bf16[30,256]{1,0:T(8,128)(2,1)S(1)}, u32[]{:S(2)}, u32[]{:S(2)}) collective-permute-start(bf16[30,256]{1,0:T(8,128)(2,1)S(1)} %slice.271), channel_id=1, source_target_pairs={{4,0},{8,4},{12,8},{16,12},{20,16},{24,20},{28,24},{5,1},{9,5},{13... | collective-permute-start | bytes 46088 | tf_op jit(solution)/shard_map/ppermute | solution.py:18
Sparse Core Ops, SparseCore 0:
  62.0 29.1 reduce-scatter.2
  114.9 14.8 all-gather.1
  133.2 64.2 reduce-scatter.4
where the time goes:
time: 206 us
  waiting for transfers between devices  108 us (52%)
  Pallas kernels  35.1 us (17%)
  matrix products  32 us (16%)
  between operations  14 us (7%)
  starting transfers between devices  7.1 us (3%)
  other arithmetic  5.7 us (3%)
  local copies, waits for them, and re-layouts  3.39 us (2%)
    reduce_scatter x1, waiting for transfers between devices, paired_body(): lax.psum_scatter(dot(mid_grad, activated, 0, 0).astype(jnp.bfloat16), 'sp...  49 us
    pallas_call x1, Pallas kernels, dispatch(): pl.pallas_call(dispatch_kernel, out_shape=(rows, rows, jax.ShapeDtypeStru...  35.1 us
    dot_general x14, matrix products, dot(): lax.dot_general(left, right, (((left_dim,), (right_dim,)), ((), ())), pre...  32 us
    reduce_scatter x1, waiting for transfers between devices, paired_body(): lax.psum_scatter(partial_value, 'tp', scatter_dimension=1, tiled=True)  29.4 us
    all_to_all x1, waiting for transfers between devices, paired_body(): lax.all_to_all(summed.reshape(experts, slots, width), 'sp', split_axis=0,...  15.6 us
    all_gather x1, waiting for transfers between devices, paired_body(): mid_grad = lax.all_gather(mid_part, 'tp', axis=1, tiled=True)  9.91 us
    all_to_all x1, starting transfers between devices, paired_body(): lax.all_to_all(summed.reshape(experts, slots, width), 'sp', split_axis=0,...  5.51 us
    ppermute x1, waiting for transfers between devices, passed_along(): lax.ppermute(value, axis, [(source, source + steps) for source in range(i...  4.31 us
  transfers between devices with their start and end apart: 5, of which 5 were waited for; matrix products, arithmetic and copies ran while one was open for 7% of the time, Pallas kernels for 0%

commit v1 on v0

--- a/solution.py
+++ b/solution.py
@@ -289,6 +289,210 @@
     )(send_m, send_c, send_w)
 
 
+def neighbours():
+    sp, tp = lax.axis_index("sp"), lax.axis_index("tp")
+    plane, side = sp // TOP, sp % TOP
+    row, core = tp // 2, tp % 2
+    across = (TOP * plane + 1 - side, tp)
+    along = (sp, 2 * (1 - row) + core)
+    partner = (sp, 2 * row + 1 - core)
+    return plane, side, row, core, across, along, partner
+
+
+def greet(targets):
+    barrier = pltpu.get_barrier_semaphore()
+    for target in targets:
+        pl.semaphore_signal(barrier, inc=1, device_id=target, device_id_type=MESH)
+    pl.semaphore_wait(barrier, len(targets))
+
+
+def wide(value):
+    return value.astype(jnp.float32)
+
+
+def give_back_kernel(
+    part, pick, cot, out, pair_in, pair_sum, in_y, in_x, sum_y, sum_x, last_x, last_y, total, back,
+    s_sem, r_sem, g_sem
+):
+    planes, _, width = back.shape
+    half = width // 2
+    plane, side, row, core, across, along, partner = neighbours()
+    tp = 2 * row + core
+    tp_other = 2 * (1 - row) + core
+    greet(
+        [across, along, partner]
+        + [(TOP * ((plane + k) % planes) + side, tp) for k in range(1, planes)]
+    )
+    copies = []
+    arrivals = {}
+
+    def remote(source, target_ref, sems, kind, k, device):
+        copy = pltpu.make_async_remote_copy(
+            src_ref=source,
+            dst_ref=target_ref,
+            send_sem=sems[0],
+            recv_sem=sems[1],
+            device_id=device,
+            device_id_type=MESH,
+        )
+        copy.start()
+        copies.append(copy)
+        arrivals[kind, k] = copy
+
+    def sems(kind, k):
+        return s_sem.at[kind, k], r_sem.at[kind, k]
+
+    def columns(quarter):
+        return pl.ds(pl.multiple_of(quarter * width, width), width)
+
+    rows_of = [TOP * ((plane + k + 1) % planes) for k in range(planes)]
+    for k in range(planes):
+        for j in range(2):
+            quarter = 2 * (row if j == 0 else 1 - row) + 1 - core
+            remote(
+                part.at[pl.ds(rows_of[k], TOP), :, columns(quarter)],
+                pair_in.at[k, j], sems(j, k), j, k, partner,
+            )
+    low, high = pl.ds(0, half), pl.ds(half, half)
+    for step in range(planes + 2):
+        k = step
+        if k < planes:
+            for j, quarter in ((0, tp), (1, tp_other)):
+                arrivals[j, k].wait_recv()
+                pair_sum[k, j] = (
+                    wide(part[pl.ds(rows_of[k], TOP), :, columns(quarter)]) + wide(pair_in[k, j])
+                ).astype(out.dtype)
+            remote(pair_sum.at[k, 1, :, :, low], in_y.at[k], sems(2, k), 2, k, along)
+            remote(pair_sum.at[k, :, 1 - side, :, high], in_x.at[k], sems(3, k), 3, k, across)
+        k = step - 1
+        if 0 <= k < planes:
+            arrivals[2, k].wait_recv()
+            sum_y[k] = (wide(pair_sum[k, 0, :, :, low]) + wide(in_y[k])).astype(out.dtype)
+            remote(sum_y.at[k, 1 - side], last_x.at[k], sems(4, k), 4, k, across)
+            arrivals[3, k].wait_recv()
+            sum_x[k] = (wide(pair_sum[k, :, side, :, high]) + wide(in_x[k])).astype(out.dtype)
+            remote(sum_x.at[k, 1], last_y.at[k], sems(5, k), 5, k, along)
+        k = step - 2
+        if 0 <= k < planes:
+            arrivals[4, k].wait_recv()
+            arrivals[5, k].wait_recv()
+            total[k, :, low] = (wide(sum_y[k, side]) + wide(last_x[k])).astype(out.dtype)
+            total[k, :, high] = (wide(sum_x[k, 0]) + wide(last_y[k])).astype(out.dtype)
+            if k < planes - 1:
+                to = (TOP * ((plane + k + 1) % planes) + side, tp)
+                remote(total.at[k], back.at[plane], sems(6, k), 6, k, to)
+    moe = jnp.dot(pick[plane], total[planes - 1], preferred_element_type=jnp.float32)
+    for k in range(planes - 1):
+        arrivals[6, k].wait_recv()
+        source = (plane + planes - k - 1) % planes
+        moe += jnp.dot(pick[source], back[source], preferred_element_type=jnp.float32)
+    out[:, columns(tp)] = (wide(cot[...]) + moe).astype(out.dtype)
+    mine = out.at[:, columns(tp)]
+    remote(mine, mine, (g_sem.at[0, 0], g_sem.at[1, 0]), 7, 0, along)
+    remote(mine, mine, (g_sem.at[0, 1], g_sem.at[1, 1]), 7, 1, partner)
+    arrivals[7, 0].wait_recv()
+    theirs = out.at[:, columns(tp_other)]
+    remote(theirs, theirs, (g_sem.at[0, 2], g_sem.at[1, 2]), 7, 2, partner)
+    arrivals[7, 1].wait_recv()
+    arrivals[7, 2].wait_recv()
+    for copy in copies:
+        copy.wait_send()
+
+
+def give_back(part, pick, cot):
+    planes, token_count, slots = pick.shape
+    width = cot.shape[1]
+    half = width // 2
+    vmem = pl.BlockSpec(memory_space=pltpu.VMEM)
+    dtype = part.dtype
+    return pl.pallas_call(
+        give_back_kernel,
+        out_shape=jax.ShapeDtypeStruct((token_count, part.shape[2]), dtype),
+        in_specs=[vmem] * 3,
+        out_specs=vmem,
+        scratch_shapes=[
+            pltpu.VMEM((planes, 2, TOP, slots, width), dtype),
+            pltpu.VMEM((planes, 2, TOP, slots, width), dtype),
+            pltpu.VMEM((planes, TOP, slots, half), dtype),
+            pltpu.VMEM((planes, 2, slots, half), dtype),
+            pltpu.VMEM((planes, TOP, slots, half), dtype),
+            pltpu.VMEM((planes, 2, slots, half), dtype),
+            pltpu.VMEM((planes, slots, half), dtype),
+            pltpu.VMEM((planes, slots, half), dtype),
+            pltpu.VMEM((planes, slots, width), dtype),
+            pltpu.VMEM((planes, slots, width), dtype),
+            pltpu.SemaphoreType.DMA((7, planes)),
+            pltpu.SemaphoreType.DMA((7, planes)),
+            pltpu.SemaphoreType.DMA((2, 3)),
+        ],
+        compiler_params=pltpu.CompilerParams(
+            collective_id=1, has_side_effects=True, vmem_limit_bytes=40 * 1024 * 1024
+        ),
+        name="give_back",
+    )(part, pick, cot)
+
+
+def reduce_kernel(prod, out, in_x, side_sum, in_z, s_sem, r_sem):
+    planes = in_x.shape[0]
+    plane, side, row, core, across, _, _ = neighbours()
+    tp = 2 * row + core
+    to = [(TOP * ((plane + k + 1) % planes) + side, tp) for k in range(planes - 1)]
+    greet([across] + to)
+
+    def remote(source, target_ref, kind, k, device):
+        copy = pltpu.make_async_remote_copy(
+            src_ref=source,
+            dst_ref=target_ref,
+            send_sem=s_sem.at[kind, k],
+            recv_sem=r_sem.at[kind, k],
+            device_id=device,
+            device_id_type=MESH,
+        )
+        copy.start()
+        return copy
+
+    rows_of = [TOP * ((plane + k + 1) % planes) for k in range(planes)]
+    crossing = [
+        remote(prod.at[rows_of[k] + 1 - side], in_x.at[k], 0, k, across) for k in range(planes)
+    ]
+    climbing = []
+    for k in range(planes):
+        crossing[k].wait_recv()
+        both = wide(prod[rows_of[k] + side]) + wide(in_x[k])
+        if k < planes - 1:
+            side_sum[k] = both.astype(prod.dtype)
+            climbing.append(remote(side_sum.at[k], in_z.at[k], 1, k, to[k]))
+    for k in range(planes - 1):
+        climbing[k].wait_recv()
+        both += wide(in_z[k])
+    out[...] = both
+    for copy in crossing + climbing:
+        copy.wait_send()
+
+
+def reduce_rows(prod):
+    blocks, rows, width = prod.shape
+    planes = blocks // TOP
+    vmem = pl.BlockSpec(memory_space=pltpu.VMEM)
+    return pl.pallas_call(
+        reduce_kernel,
+        out_shape=jax.ShapeDtypeStruct((rows, width), jnp.float32),
+        in_specs=[vmem],
+        out_specs=vmem,
+        scratch_shapes=[
+            pltpu.VMEM((planes, rows, width), prod.dtype),
+            pltpu.VMEM((planes - 1, rows, width), prod.dtype),
+            pltpu.VMEM((planes - 1, rows, width), prod.dtype),
+            pltpu.SemaphoreType.DMA((2, planes)),
+            pltpu.SemaphoreType.DMA((2, planes)),
+        ],
+        compiler_params=pltpu.CompilerParams(
+            collective_id=2, has_side_effects=True, vmem_limit_bytes=32 * 1024 * 1024
+        ),
+        name="reduce_rows",
+    )(prod)
+
+
 def dot(left, right, left_dim, right_dim):
     return lax.dot_general(
         left, right, (((left_dim,), (right_dim,)), ((), ())), preferred_element_type=jnp.float32
@@ -360,19 +564,13 @@
     partial_value = (dot(gate_grad, gate_mat, 1, 1) + dot(up_grad, up_mat, 1, 1)).astype(
         jnp.bfloat16
     )
-    summed = lax.psum_scatter(partial_value, "tp", scatter_dimension=1, tiled=True)
-    returned = lax.all_to_all(
-        summed.reshape(experts, slots, width), "sp", split_axis=0, concat_axis=0, tiled=True
-    )
-    pick_each = jnp.repeat(pick.reshape(GROUPS, 1, slots, token_count), TOP, axis=1)
-    moe_grad = dot(
-        pick_each.reshape(experts * slots, token_count),
-        returned.reshape(experts * slots, width),
-        0,
-        0,
-    )
-    mid_part = (own_cot.astype(jnp.float32) + moe_grad).astype(jnp.bfloat16)
-    mid_grad = lax.all_gather(mid_part, "tp", axis=1, tiled=True)
+    own_slot = slot[None, :, None] == (
+        slots * jnp.arange(GROUPS, dtype=jnp.int32)[:, None, None]
+        + jnp.arange(slots, dtype=jnp.int32)[None, None, :]
+    )
+    mid_grad = give_back(
+        partial_value.reshape(experts, slots, D), own_slot.astype(jnp.bfloat16), own_cot
+    )
     grad_down = dot(hidden, seeds, 0, 0).astype(jnp.bfloat16)
     grad_gate = dot(inputs, gate_grad, 0, 0).astype(jnp.bfloat16)
     grad_up = dot(inputs, up_grad, 0, 0).astype(jnp.bfloat16)
@@ -389,12 +587,9 @@
             + conv_taps[lag_index].astype(jnp.float32)[None, :]
             * extended[lag_index : lag_index + token_count]
         )
-    grad_proj = lax.psum_scatter(
-        dot(mid_grad, activated, 0, 0).astype(jnp.bfloat16),
-        "sp",
-        scatter_dimension=0,
-        tiled=True,
-    ).astype(jnp.float32)
+    grad_proj = reduce_rows(
+        dot(mid_grad, activated, 0, 0).astype(jnp.bfloat16).reshape(experts, D // experts, -1)
+    )
     return (grad_gate[None], grad_up[None], grad_down[None], grad_proj, conv_input_grad)
 
 

time: 206 us -> 116 us (0.56)
  waiting for transfers between devices: 108 us -> 0.01 us
  Pallas kernels: 35.1 us -> 81.9 us
  between operations: 14 us -> 0.95 us
  matrix products: 32 us -> 21.5 us
  starting transfers between devices: 7.1 us -> 1.6 us
    reduce_scatter x2 -> x0, waiting for transfers between devices: 78.3 us -> none  [the longest x1 49 us: paired_body(): lax.psum_scatter(dot(mid_grad, activated, 0, 0).astype(jnp.bfloat16), 'sp...]
    pallas_call x0 -> x2, Pallas kernels: none -> 46.7 us  [the longest x1 25.4 us: give_back(): pl.pallas_call(give_back_kernel, out_shape=jax.ShapeDtypeStruct((token_co...]
    all_to_all x1 -> x0, waiting for transfers between devices: 15.6 us -> none  [paired_body(): lax.all_to_all(summed.reshape(experts, slots, width), 'sp', split_axis=0,...]
    dot_general x14 -> x13, matrix products: 32 us -> 21.5 us  [dot(): lax.dot_general(left, right, (((left_dim,), (right_dim,)), ((), ())), pre...]
    all_gather x1 -> x0, waiting for transfers between devices: 9.91 us -> none  [paired_body(): mid_grad = lax.all_gather(mid_part, 'tp', axis=1, tiled=True)]
    all_to_all x1 -> x0, starting transfers between devices: 5.51 us -> none  [paired_body(): lax.all_to_all(summed.reshape(experts, slots, width), 'sp', split_axis=0,...]
    ppermute x1, waiting for transfers between devices: 4.31 us -> 0.01 us  [passed_along(): lax.ppermute(value, axis, [(source, source + steps) for source in range(i...]
  transfers between devices with their start and end apart: 5 -> 1, of which waited for: 5 -> 0; matrix products, arithmetic and copies ran while one was open for 7% -> 9% of each run, Pallas kernels for 0% -> 19%
where the time goes in v1:
time: 116 us; the launch traced here: 115 us
  Pallas kernels  81.9 us (71%)
  matrix products  21.5 us (19%)
  local copies, waits for them, and re-layouts  5.08 us (4%)
  other arithmetic  4.16 us (4%)
  starting transfers between devices  1.6 us (1%)
    pallas_call x1, Pallas kernels, dispatch(): pl.pallas_call(dispatch_kernel, out_shape=(rows, rows, jax.ShapeDtypeStru...  35.1 us
    pallas_call x1, Pallas kernels, give_back(): pl.pallas_call(give_back_kernel, out_shape=jax.ShapeDtypeStruct((token_co...  25.4 us
    dot_general x13, matrix products, dot(): lax.dot_general(left, right, (((left_dim,), (right_dim,)), ((), ())), pre...  21.5 us
    pallas_call x1, Pallas kernels, reduce_rows(): pl.pallas_call(reduce_kernel, out_shape=jax.ShapeDtypeStruct((rows, width...  21.3 us
    unnamed x25, local copies, waits for them, and re-layouts  2.34 us
  transfers between devices with their start and end apart: 1, of which 0 were waited for; matrix products, arithmetic and copies ran while one was open for 9% of the time, Pallas kernels for 19%

profile of v1, /device:TPU:0, one launch (start us, length us, event | category | flops | bytes accessed | tf_op | source)
XLA Modules:
  0.0 115.2 jit_solution(17406986580103898616)
XLA Ops:
  0.6 0.0 copy-start
  0.7 0.8 slice.204
  1.5 0.2 fusion.14
  1.7 1.0 constant_dynamic-slice_fusion.1.cot
  2.7 1.2 %convolution_convert_fusion.5 = bf16[288,512]{1,0:T(8,128)(2,1)S(1)} fusion(bf16[256,2048]{1,0:T(8,128)(2,1)} %param.10, s32[]{:T(128)S(6)} %select_n.85, s32[256]{0:T(256)S(1)} %compare_select_fusion), kind=kOutput, calls=%fused_computation.19 | convolution fusion | flops 75718656 | bytes 558084 | tf_op jit(solution)/shard_map/dot_general | solution.py:497
  3.9 0.2 convolution_convert_fusion.4
  4.1 0.8 fusion.64
  4.9 0.2 select_reduce_fusion.1
  5.1 0.1 reshape.191
  5.2 0.1 reshape.190
  5.3 35.1 %dispatch.1 = (bf16[8,72,2048]{2,1,0:T(8,128)(2,1)S(1)}, bf16[8,72,2048]{2,1,0:T(8,128)(2,1)S(1)}, f32[8,8,128]{2,1,0:T(8,128)S(1)}) custom-call(bf16[4,72,512]{2,1,0:T(8,128)(2,1)S(1)} %bitcast.78, bf16[4,72,512]{2,1,0:T(8,128)(2,1)S(1)} %bitcast.79, f32[4,8,128]{2,1,0:T(8,128)S(1)} %select_maximum_fusion.send_w), custom_call_target="tpu_custom_call" | custom-call | tf_op jit(solution)/shard_map/dispatch/pallas_call | solution.py:274
  40.4 0.0 copy-start.1
  40.4 0.0 copy-start.2
  40.5 0.0 copy-start.4
  40.5 2.4 %fusion.5 = f32[576,512]{1,0:T(8,128)} fusion(bf16[576,2048]{1,0:T(8,128)(2,1)S(1)} %bitcast.81, bf16[1,2048,512]{2,1,0:T(8,128)(2,1)S(1)} %copy-done), kind=kOutput, calls=%fused_computation.11 | convolution fusion | flops 1207959552 | bytes 5636096 | tf_op jit(solution)/shard_map/dot_general | solution.py:497
  42.9 0.0 copy-done.1
  42.9 0.3 copy-done.2
  43.1 0.5 copy-done.4
  43.6 2.4 %fusion.8 = f32[576,512]{1,0:T(8,128)} fusion(bf16[576,2048]{1,0:T(8,128)(2,1)S(1)} %bitcast.82, bf16[1,2048,512]{2,1,0:T(8,128)(2,1)S(1)} %copy-done.4), kind=kOutput, calls=%fused_computation.14 | convolution fusion | flops 1207959552 | bytes 5636096 | tf_op jit(solution)/shard_map/dot_general | solution.py:497
  46.0 0.0 copy-start.10
  46.1 0.0 copy-start.11
  46.1 2.3 %multiply_convert_fusion = bf16[8,72,2048]{2,1,0:T(8,128)(2,1)S(1)} fusion(bf16[8,72,2048]{2,1,0:T(8,128)(2,1)} %copy-done.1, f32[8,72]{1,0:T(8,128)S(1)} %bitcast.90), kind=kLoop, calls=%fused_computation.1 | loop fusion | flops 3538944 | bytes 4720896 | tf_op jit(solution)/shard_map/convert_element_type | solution.py:551
  48.3 0.3 copy-done.10
  48.6 0.4 copy-done.11
  49.0 1.7 %multiply_convert_fusion.2 = (bf16[576,512]{1,0:T(8,128)(2,1)S(1)}, bf16[576,512]{1,0:T(8,128)(2,1)S(1)}) fusion(f32[576,512]{1,0:T(8,128)S(1)} %copy-done.10, f32[576,512]{1,0:T(8,128)S(1)} %copy-done.11, bf16[576,2048]{1,0:T(8,128)(2,1)S(1)} %bitcast.85, bf16[1,512,2048]{2,1,0:T(8,128)(2,1)S(1)} %copy-done.7), kind=kOutput, calls=%fused_computation.21 | convolution fusion | flops 1211793408 | bytes 7995392 | tf_op jit(solution)/shard_map/dot_general | solution.py:497
  50.8 0.0 copy-start.5
  50.8 1.4 %fusion.3 = f32[576,2048]{1,0:T(8,128)S(1)} fusion(bf16[576,512]{1,0:T(8,128)(2,1)S(1)} %get-tuple-element.14, bf16[1,2048,512]{2,1,0:T(8,128)(2,1)S(1)} %copy-done), kind=kOutput, calls=%fused_computation.9 | convolution fusion | flops 1207959552 | bytes 7405568 | tf_op jit(solution)/shard_map/dot_general | solution.py:497
  52.2 0.1 iota_add_fusion
  52.3 0.1 compare_convert_fusion.pick
  52.4 1.4 %add_convert_fusion = bf16[576,2048]{1,0:T(8,128)(2,1)S(1)} fusion(f32[576,2048]{1,0:T(8,128)S(1)} %fusion.3, bf16[576,512]{1,0:T(8,128)(2,1)S(1)} %get-tuple-element.13, bf16[1,2048,512]{2,1,0:T(8,128)(2,1)S(1)} %copy-done.5), kind=kOutput, calls=%fused_computation | convolution fusion | flops 1210318848 | bytes 9764864 | tf_op jit(solution)/shard_map/dot_general | solution.py:497
  53.8 0.0 copy-start.8
  53.8 0.0 copy-start.9
  53.8 25.4 %give_back.1 = bf16[256,2048]{1,0:T(8,128)(2,1)S(1)} custom-call(bf16[8,72,2048]{2,1,0:T(8,128)(2,1)S(1)} %bitcast.77, bf16[4,256,72]{2,1,0:T(8,128)(2,1)S(1)} %compare_convert_fusion.pick, bf16[256,512]{1,0:T(8,128)(2,1)S(1)} %constant_dynamic-slice_fusion.1.cot), custom_call_target="tpu_custom_call" | custom-call | tf_op jit(solution)/shard_map/give_back/pallas_call | solution.py:408
  79.3 0.0 copy-done.8
  79.3 0.0 copy-done.9
  79.3 0.0 copy-start.3
  79.3 0.5 fusion.13
  79.8 1.6 %collective-permute-start = (bf16[30,256]{1,0:T(8,128)(2,1)S(1)}, bf16[30,256]{1,0:T(8,128)(2,1)S(1)}, u32[]{:S(2)}, u32[]{:S(2)}) collective-permute-start(bf16[30,256]{1,0:T(8,128)(2,1)S(1)} %slice.271), channel_id=1, source_target_pairs={{4,0},{8,4},{12,8},{16,12},{20,16},{24,20},{28,24},{5,1},{9,5},{13... | collective-permute-start | bytes 46088 | tf_op jit(solution)/shard_map/ppermute | solution.py:18
  81.4 0.0 copy-done.3
  81.4 3.2 %fusion = bf16[1,2048,512]{2,1,0:T(8,128)(2,1)} fusion(bf16[576,2048]{1,0:T(8,128)(2,1)S(1)} %bitcast.83, bf16[576,512]{1,0:T(8,128)(2,1)S(1)} %get-tuple-element.14), kind=kOutput, calls=%fused_computation.5 | convolution fusion | flops 1209008128 | bytes 5046272 | tf_op jit(solution)/shard_map/dot_general | solution.py:497
  84.6 3.2 %fusion.1 = bf16[1,2048,512]{2,1,0:T(8,128)(2,1)} fusion(bf16[576,2048]{1,0:T(8,128)(2,1)S(1)} %bitcast.84, bf16[576,512]{1,0:T(8,128)(2,1)S(1)} %get-tuple-element.13), kind=kOutput, calls=%fused_computation.6 | convolution fusion | flops 1209008128 | bytes 5046272 | tf_op jit(solution)/shard_map/dot_general | solution.py:497
  87.7 3.2 %fusion.2 = bf16[1,512,2048]{2,1,0:T(8,128)(2,1)} fusion(bf16[576,2048]{1,0:T(8,128)(2,1)S(1)} %bitcast.86, f32[576,512]{1,0:T(8,128)S(1)} %copy-done.11, f32[576,512]{1,0:T(8,128)S(1)} %copy-done.10), kind=kOutput, calls=%fused_computation.7 | convolution fusion | flops 1210777600 | bytes 6815744 | tf_op jit(solution)/shard_map/dot_general | solution.py:497
  90.9 0.5 convolution_convert_fusion.3
  91.5 0.2 copy-done.6
  91.7 21.3 %reduce_rows.1 = f32[256,256]{1,0:T(8,128)S(1)} custom-call(bf16[8,256,256]{2,1,0:T(8,128)(2,1)S(1)} %bitcast.80), custom_call_target="tpu_custom_call" | custom-call | tf_op jit(solution)/shard_map/reduce_rows/pallas_call | solution.py:477
  113.0 0.0 collective-permute-done
  113.1 1.4 %fusion.21 = f32[256,256]{1,0:T(8,128)} fusion(f32[286,256]{1,0:T(8,128)S(1)} %maximum_convert_fusion, f32[256]{0:T(256)S(1)} %bitcast.122, f32[256]{0:T(256)S(1)} %bitcast.123, f32[256]{0:T(256)S(1)} %bitcast.94, f32[256]{0:T(256)S(1)} %bitcast.95, f32[256]{0:T(256)S(1)} %bitcast.96, f32[256]{0:T(256)S(1)} %bitcast.97, f32[256]{0:T(256)S(1)} %bitcast.98, ...), kind=kLoop, calls=%fused_computation.43 | loop fusion | flops 3997696 | bytes 8420352 | tf_op jit(solution)/shard_map/add | solution.py:586
  114.5 0.7 copy.16
  (15 shorter events, 0.1 us)
Async XLA Ops:
  0.6 39.8 %copy-start = (bf16[1,2048,512]{2,1,0:T(8,128)(2,1)S(1)}, bf16[1,2048,512]{2,1,0:T(8,128)(2,1)}, u32[]{:S(2)}) copy-start(bf16[1,2048,512]{2,1,0:T(8,128)(2,1)} %param.16) | copy-start | bytes 6291460
  40.4 2.4 %copy-start.1 = (bf16[8,72,2048]{2,1,0:T(8,128)(2,1)}, bf16[8,72,2048]{2,1,0:T(8,128)(2,1)S(1)}, u32[]{:S(2)}) copy-start(bf16[8,72,2048]{2,1,0:T(8,128)(2,1)S(1)} %get-tuple-element.10) | copy-start | bytes 7077892
  40.4 2.7 %copy-start.2 = (bf16[8,72,2048]{2,1,0:T(8,128)(2,1)}, bf16[8,72,2048]{2,1,0:T(8,128)(2,1)S(1)}, u32[]{:S(2)}) copy-start(bf16[8,72,2048]{2,1,0:T(8,128)(2,1)S(1)} %get-tuple-element.8) | copy-start | bytes 7077892
  40.5 3.1 %copy-start.4 = (bf16[1,2048,512]{2,1,0:T(8,128)(2,1)S(1)}, bf16[1,2048,512]{2,1,0:T(8,128)(2,1)}, u32[]{:S(2)}) copy-start(bf16[1,2048,512]{2,1,0:T(8,128)(2,1)} %param.17) | copy-start | bytes 6291460
  46.0 2.3 %copy-start.7 = (bf16[1,512,2048]{2,1,0:T(8,128)(2,1)S(1)}, bf16[1,512,2048]{2,1,0:T(8,128)(2,1)}, u32[]{:S(2)}) copy-start(bf16[1,512,2048]{2,1,0:T(8,128)(2,1)} %param.18) | copy-start | bytes 6291460
  46.0 2.6 %copy-start.10 = (f32[576,512]{1,0:T(8,128)S(1)}, f32[576,512]{1,0:T(8,128)}, u32[]{:S(2)}) copy-start(f32[576,512]{1,0:T(8,128)} %fusion.5) | copy-start | bytes 3538948
  46.1 2.9 %copy-start.11 = (f32[576,512]{1,0:T(8,128)S(1)}, f32[576,512]{1,0:T(8,128)}, u32[]{:S(2)}) copy-start(f32[576,512]{1,0:T(8,128)} %fusion.8) | copy-start | bytes 3538948
  50.8 1.6 %copy-start.5 = (bf16[1,2048,512]{2,1,0:T(8,128)(2,1)S(1)}, bf16[1,2048,512]{2,1,0:T(8,128)(2,1)}, u32[]{:S(2)}) copy-start(bf16[1,2048,512]{2,1,0:T(8,128)(2,1)} %param.17) | copy-start | bytes 6291460
  53.8 25.4 %copy-start.8 = (bf16[256,2048]{1,0:T(8,128)(2,1)S(1)}, bf16[256,2048]{1,0:T(8,128)(2,1)}, u32[]{:S(2)}) copy-start(bf16[256,2048]{1,0:T(8,128)(2,1)} %param.13) | copy-start | bytes 3145732
  53.8 25.4 %copy-start.9 = (bf16[256,256]{1,0:T(8,128)(2,1)S(1)}, bf16[256,256]{1,0:T(8,128)(2,1)}, u32[]{:S(2)}) copy-start(bf16[256,256]{1,0:T(8,128)(2,1)} %param.11) | copy-start | bytes 393220
  79.3 2.1 %copy-start.3 = (bf16[8,72,2048]{2,1,0:T(8,128)(2,1)S(1)}, bf16[8,72,2048]{2,1,0:T(8,128)(2,1)}, u32[]{:S(2)}) copy-start(bf16[8,72,2048]{2,1,0:T(8,128)(2,1)} %copy-done.2) | copy-start | bytes 7077892
  79.8 33.2 %collective-permute-start = (bf16[30,256]{1,0:T(8,128)(2,1)S(1)}, bf16[30,256]{1,0:T(8,128)(2,1)S(1)}, u32[]{:S(2)}, u32[]{:S(2)}) collective-permute-start(bf16[30,256]{1,0:T(8,128)(2,1)S(1)} %slice.271), channel_id=1, source_target_pairs={{4,0},{8,4},{12,8},{16,12},{20,16},{24,20},{28,24},{5,1},{9,5},{13... | collective-permute-start | bytes 46088 | tf_op jit(solution)/shard_map/ppermute | solution.py:18
  90.9 0.7 copy-start.6

commit v2 on v0

--- a/solution.py
+++ b/solution.py
@@ -144,80 +144,117 @@
     return (grad_gate[None], grad_up[None], grad_down[None], grad_proj, conv_input_grad)
 
 
-def dispatch_kernel(send_m, send_c, send_w, out_m, out_c, out_w, s_sem, r_sem, w_sem, l_sem):
+def neighbours():
     sp, tp = lax.axis_index("sp"), lax.axis_index("tp")
-    planes, slots, width = send_m.shape
     plane, side = sp // TOP, sp % TOP
     row, core = tp // 2, tp % 2
     across = (TOP * plane + 1 - side, tp)
     along = (sp, 2 * (1 - row) + core)
     partner = (sp, 2 * row + 1 - core)
-
+    return plane, side, row, core, across, along, partner
+
+
+def greet(targets):
     barrier = pltpu.get_barrier_semaphore()
-    targets = [across, along, partner]
-    targets += [(TOP * ((plane + k) % planes) + side, tp) for k in range(1, planes)]
     for target in targets:
         pl.semaphore_signal(barrier, inc=1, device_id=target, device_id_type=MESH)
     pl.semaphore_wait(barrier, len(targets))
 
+
+def wide(value):
+    return value.astype(jnp.float32)
+
+
+def exchange_kernel(
+    send_m, send_c, send_w, pick, cot, gate_hbm, up_hbm, down_hbm,
+    out, out_m, out_seed, out_hidden, out_gate, out_up,
+    out_c, out_w, gate_w, up_w, down_w, part,
+    pair_in, pair_sum, in_y, in_x, sum_y, sum_x, last_x, last_y, total, back,
+    s_sem, r_sem, w_sem, l_sem, s2_sem, r2_sem, g_sem
+):
+    planes, slots, width = send_m.shape
+    half = width // 2
+    plane, side, row, core, across, along, partner = neighbours()
+    own = TOP * plane + side
+    tp = 2 * row + core
+    other = 2 * (1 - row) + core
     sends = (send_m, send_c)
     outs = (out_m, out_c)
 
+    loads = [
+        pltpu.make_async_copy(source, target, l_sem.at[3 + i])
+        for i, (source, target) in enumerate(
+            ((gate_hbm, gate_w), (up_hbm, up_w), (down_hbm, down_w))
+        )
+    ]
+    for load in loads:
+        load.start()
+    greet(
+        [across, along, partner]
+        + [(TOP * ((plane + k) % planes) + side, tp) for k in range(1, planes)]
+    )
+    copies = []
+    arrivals = {}
+
+    def columns(quarter):
+        return pl.ds(pl.multiple_of(quarter * width, width), width)
+
     def place(array, block, quarter):
-        return outs[array].at[block, :, pl.ds(pl.multiple_of(quarter * width, width), width)]
-
-    def remote(source, target_ref, kind, k, array, device):
-        return pltpu.make_async_remote_copy(
+        return outs[array].at[block, :, columns(quarter)]
+
+    def remote(source, target_ref, send_sem, recv_sem, key, device):
+        copy = pltpu.make_async_remote_copy(
             src_ref=source,
             dst_ref=target_ref,
-            send_sem=s_sem.at[kind, k, array],
-            recv_sem=r_sem.at[kind, k, array],
+            send_sem=send_sem,
+            recv_sem=recv_sem,
             device_id=device,
             device_id_type=MESH,
         )
+        copy.start()
+        copies.append(copy)
+        arrivals[key] = copy
+
+    def move(source, target_ref, kind, k, array, device):
+        remote(
+            source, target_ref, s_sem.at[kind, k, array], r_sem.at[kind, k, array],
+            (kind, k, array), device,
+        )
 
     def weights(source, block, kind, k, device):
-        return pltpu.make_async_remote_copy(
-            src_ref=source,
-            dst_ref=out_w.at[block],
-            send_sem=w_sem.at[0, kind, k],
-            recv_sem=w_sem.at[1, kind, k],
-            device_id=device,
-            device_id_type=MESH,
-        )
-
-    copies = []
-    arrivals = {}
-    own = TOP * plane + side
+        remote(
+            source, out_w.at[block], w_sem.at[0, kind, k], w_sem.at[1, kind, k],
+            (kind, k, 2), device,
+        )
+
+    def give(source, target_ref, kind, k, device):
+        remote(
+            source, target_ref, s2_sem.at[kind, k], r2_sem.at[kind, k], ("give", kind, k), device
+        )
+
+    def got(kind, k):
+        arrivals["give", kind, k].wait_recv()
+
     for k in range(1, planes):
         to = (plane - k + planes) % planes
         device = (TOP * to + side, tp)
         for array in range(2):
-            copy = remote(sends[array].at[to], place(array, own, tp), 0, k, array, device)
-            copy.start()
-            copies.append(copy)
-            arrivals[0, k, array] = copy
-        copy = weights(send_w.at[to], own, 0, k, device)
-        copy.start()
-        copies.append(copy)
-        arrivals[0, k, 2] = copy
-
-    local = []
-    for array in range(2):
-        local.append(pltpu.make_async_copy(sends[array].at[plane], place(array, own, tp), l_sem.at[array]))
+            move(sends[array].at[to], place(array, own, tp), 0, k, array, device)
+        weights(send_w.at[to], own, 0, k, device)
+    local = [
+        pltpu.make_async_copy(sends[array].at[plane], place(array, own, tp), l_sem.at[array])
+        for array in range(2)
+    ]
     local.append(pltpu.make_async_copy(send_w.at[plane], out_w.at[own], l_sem.at[2]))
     for copy in local:
         copy.start()
 
     def forward(kind, k, array, block, quarter, device, source=None):
         ref = place(array, block, quarter)
-        copy = remote(ref if source is None else source, ref, kind, k, array, device)
-        copy.start()
-        copies.append(copy)
-        arrivals[kind, k, array] = copy
-
-    other = 2 * (1 - row) + core
-    for step in range(planes + 2):
+        move(ref if source is None else source, ref, kind, k, array, device)
+
+    low, high = pl.ds(0, half), pl.ds(half, half)
+    for step in range(planes + 6):
         k = step
         if k < planes:
             block = TOP * ((plane + k) % planes) + side
@@ -230,11 +267,7 @@
                 forward(3, k, array, block, tp, partner, source)
             if k > 0:
                 arrivals[0, k, 2].wait_recv()
-            source = send_w.at[plane] if k == 0 else out_w.at[block]
-            copy = weights(source, block, 1, k, across)
-            copy.start()
-            copies.append(copy)
-            arrivals[1, k, 2] = copy
+            weights(send_w.at[plane] if k == 0 else out_w.at[block], block, 1, k, across)
         k = step - 1
         if 0 <= k < planes:
             mine = TOP * ((plane + k) % planes) + side
@@ -256,37 +289,199 @@
             for array in range(2):
                 arrivals[4, k, array].wait_recv()
                 forward(7, k, array, theirs, other, partner)
-    for k in range(planes):
-        for array in range(2):
-            for kind in (3, 5, 6, 7):
-                arrivals[kind, k, array].wait_recv()
+        k = step - 3
+        if 0 <= k < planes:
+            base = TOP * ((plane + k) % planes)
+            if k == 0:
+                for copy in local + loads:
+                    copy.wait()
+            for array in range(2):
+                for kind in (3, 5, 6, 7):
+                    arrivals[kind, k, array].wait_recv()
+            inputs = []
+            seeds = []
+            for s in range(TOP):
+                table = jnp.transpose(out_w[base + s])[:slots]
+                weight = jnp.where(side == 0, table[:, 0:1], table[:, 1:2])
+                inputs.append(wide(out_m[base + s]))
+                seeds.append(weight * wide(out_c[base + s]))
+                out_seed[base + s] = seeds[s].astype(out.dtype)
+            inputs = jnp.concatenate(inputs, axis=0).astype(out.dtype)
+            seeds = jnp.concatenate(seeds, axis=0).astype(out.dtype)
+            gate_pre = dot(inputs, gate_w[...], 1, 0)
+            up_pre = dot(inputs, up_w[...], 1, 0)
+            hidden_grad = dot(seeds, down_w[...], 1, 1)
+            sig = jax.nn.sigmoid(gate_pre)
+            gate_act = gate_pre * sig
+            hidden = gate_act * up_pre
+            gate_grad = hidden_grad * up_pre * (sig * (1.0 + gate_pre * (1.0 - sig)))
+            up_grad = hidden_grad * gate_act
+            sums = dot(gate_grad.astype(out.dtype), gate_w[...], 1, 1)
+            sums += dot(up_grad.astype(out.dtype), up_w[...], 1, 1)
+            for s in range(TOP):
+                rows = slice(s * slots, (s + 1) * slots)
+                part[k, s] = sums[rows].astype(out.dtype)
+                out_hidden[base + s] = hidden[rows].astype(out.dtype)
+                out_gate[base + s] = gate_grad[rows].astype(out.dtype)
+                out_up[base + s] = up_grad[rows].astype(out.dtype)
+            for j in range(2):
+                quarter = 2 * (row if j == 0 else 1 - row) + 1 - core
+                give(part.at[k, :, :, columns(quarter)], pair_in.at[k, j], j, k, partner)
+        k = step - 4
+        if 0 <= k < planes:
+            for j, quarter in ((0, tp), (1, other)):
+                got(j, k)
+                pair_sum[k, j] = (
+                    wide(part[k, :, :, columns(quarter)]) + wide(pair_in[k, j])
+                ).astype(out.dtype)
+            give(pair_sum.at[k, 1, :, :, low], in_y.at[k], 2, k, along)
+            give(pair_sum.at[k, :, 1 - side, :, high], in_x.at[k], 3, k, across)
+        k = step - 5
+        if 0 <= k < planes:
+            got(2, k)
+            sum_y[k] = (wide(pair_sum[k, 0, :, :, low]) + wide(in_y[k])).astype(out.dtype)
+            give(sum_y.at[k, 1 - side], last_x.at[k], 4, k, across)
+            got(3, k)
+            sum_x[k] = (wide(pair_sum[k, :, side, :, high]) + wide(in_x[k])).astype(out.dtype)
+            give(sum_x.at[k, 1], last_y.at[k], 5, k, along)
+        k = step - 6
+        if 0 <= k < planes:
+            got(4, k)
+            got(5, k)
+            total[k, :, low] = (wide(sum_y[k, side]) + wide(last_x[k])).astype(out.dtype)
+            total[k, :, high] = (wide(sum_x[k, 0]) + wide(last_y[k])).astype(out.dtype)
+            if k > 0:
+                to = (TOP * ((plane + k) % planes) + side, tp)
+                give(total.at[k], back.at[plane], 6, k, to)
+    moe = dot(pick[plane], total[0], 1, 0)
+    for k in range(1, planes):
+        got(6, k)
+        source = (plane + planes - k) % planes
+        moe += dot(pick[source], back[source], 1, 0)
+    out[:, columns(tp)] = (wide(cot[...]) + moe).astype(out.dtype)
+    mine = out.at[:, columns(tp)]
+    remote(mine, mine, g_sem.at[0, 0], g_sem.at[1, 0], "along", along)
+    remote(mine, mine, g_sem.at[0, 1], g_sem.at[1, 1], "partner", partner)
+    arrivals["along"].wait_recv()
+    theirs = out.at[:, columns(other)]
+    remote(theirs, theirs, g_sem.at[0, 2], g_sem.at[1, 2], "last", partner)
+    arrivals["partner"].wait_recv()
+    arrivals["last"].wait_recv()
     for copy in copies:
         copy.wait_send()
-    for copy in local:
-        copy.wait()
-
-
-def dispatch(send_m, send_c, send_w):
+
+
+def exchange(send_m, send_c, send_w, pick, cot, gate_mat, up_mat, down_mat):
     planes, slots, width = send_m.shape
-    blocks = lax.axis_size("sp")
+    token_count = cot.shape[0]
+    blocks = planes * TOP
+    wide_rows = width * lax.axis_size("tp")
+    hidden_width = down_mat.shape[0]
+    half = width // 2
+    dtype = send_m.dtype
     vmem = pl.BlockSpec(memory_space=pltpu.VMEM)
-    rows = jax.ShapeDtypeStruct((blocks, slots, width * lax.axis_size("tp")), send_m.dtype)
+    hbm = pl.BlockSpec(memory_space=pl.ANY)
+    rows = jax.ShapeDtypeStruct((blocks, slots, wide_rows), dtype)
+    units = jax.ShapeDtypeStruct((blocks, slots, hidden_width), dtype)
+    dma = pltpu.SemaphoreType.DMA
     return pl.pallas_call(
-        dispatch_kernel,
-        out_shape=(rows, rows, jax.ShapeDtypeStruct((blocks,) + send_w.shape[1:], send_w.dtype)),
-        in_specs=[vmem] * 3,
-        out_specs=(vmem, vmem, vmem),
+        exchange_kernel,
+        out_shape=(
+            jax.ShapeDtypeStruct((token_count, wide_rows), dtype), rows, rows, units, units, units
+        ),
+        in_specs=[vmem] * 5 + [hbm] * 3,
+        out_specs=(vmem,) * 6,
         scratch_shapes=[
-            pltpu.SemaphoreType.DMA((8, planes, 2)),
-            pltpu.SemaphoreType.DMA((8, planes, 2)),
-            pltpu.SemaphoreType.DMA((2, 2, planes)),
-            pltpu.SemaphoreType.DMA((3,)),
+            pltpu.VMEM((blocks, slots, wide_rows), dtype),
+            pltpu.VMEM((blocks,) + send_w.shape[1:], send_w.dtype),
+            pltpu.VMEM(gate_mat.shape, dtype),
+            pltpu.VMEM(up_mat.shape, dtype),
+            pltpu.VMEM(down_mat.shape, dtype),
+            pltpu.VMEM((planes, TOP, slots, wide_rows), dtype),
+            pltpu.VMEM((planes, 2, TOP, slots, width), dtype),
+            pltpu.VMEM((planes, 2, TOP, slots, width), dtype),
+            pltpu.VMEM((planes, TOP, slots, half), dtype),
+            pltpu.VMEM((planes, 2, slots, half), dtype),
+            pltpu.VMEM((planes, TOP, slots, half), dtype),
+            pltpu.VMEM((planes, 2, slots, half), dtype),
+            pltpu.VMEM((planes, slots, half), dtype),
+            pltpu.VMEM((planes, slots, half), dtype),
+            pltpu.VMEM((planes, slots, width), dtype),
+            pltpu.VMEM((planes, slots, width), dtype),
+            dma((8, planes, 2)),
+            dma((8, planes, 2)),
+            dma((2, 2, planes)),
+            dma((6,)),
+            dma((7, planes)),
+            dma((7, planes)),
+            dma((2, 3)),
         ],
         compiler_params=pltpu.CompilerParams(
-            collective_id=0, has_side_effects=True, vmem_limit_bytes=32 * 1024 * 1024
+            collective_id=0, has_side_effects=True, vmem_limit_bytes=56 * 1024 * 1024
         ),
-        name="dispatch",
-    )(send_m, send_c, send_w)
+        name="exchange",
+    )(send_m, send_c, send_w, pick, cot, gate_mat, up_mat, down_mat)
+
+
+def reduce_kernel(prod, out, in_x, side_sum, in_z, s_sem, r_sem):
+    planes = in_x.shape[0]
+    plane, side, row, core, across, _, _ = neighbours()
+    tp = 2 * row + core
+    to = [(TOP * ((plane + k + 1) % planes) + side, tp) for k in range(planes - 1)]
+    greet([across] + to)
+
+    def remote(source, target_ref, kind, k, device):
+        copy = pltpu.make_async_remote_copy(
+            src_ref=source,
+            dst_ref=target_ref,
+            send_sem=s_sem.at[kind, k],
+            recv_sem=r_sem.at[kind, k],
+            device_id=device,
+            device_id_type=MESH,
+        )
+        copy.start()
+        return copy
+
+    rows_of = [TOP * ((plane + k + 1) % planes) for k in range(planes)]
+    crossing = [
+        remote(prod.at[rows_of[k] + 1 - side], in_x.at[k], 0, k, across) for k in range(planes)
+    ]
+    climbing = []
+    for k in range(planes):
+        crossing[k].wait_recv()
+        both = wide(prod[rows_of[k] + side]) + wide(in_x[k])
+        if k < planes - 1:
+            side_sum[k] = both.astype(prod.dtype)
+            climbing.append(remote(side_sum.at[k], in_z.at[k], 1, k, to[k]))
+    for k in range(planes - 1):
+        climbing[k].wait_recv()
+        both += wide(in_z[k])
+    out[...] = both
+    for copy in crossing + climbing:
+        copy.wait_send()
+
+
+def reduce_rows(prod):
+    blocks, rows, width = prod.shape
+    planes = blocks // TOP
+    vmem = pl.BlockSpec(memory_space=pltpu.VMEM)
+    return pl.pallas_call(
+        reduce_kernel,
+        out_shape=jax.ShapeDtypeStruct((rows, width), jnp.float32),
+        in_specs=[vmem],
+        out_specs=vmem,
+        scratch_shapes=[
+            pltpu.VMEM((planes, rows, width), prod.dtype),
+            pltpu.VMEM((planes - 1, rows, width), prod.dtype),
+            pltpu.VMEM((planes - 1, rows, width), prod.dtype),
+            pltpu.SemaphoreType.DMA((2, planes)),
+            pltpu.SemaphoreType.DMA((2, planes)),
+        ],
+        compiler_params=pltpu.CompilerParams(
+            collective_id=2, has_side_effects=True, vmem_limit_bytes=32 * 1024 * 1024
+        ),
+        name="reduce_rows",
+    )(prod)
 
 
 def dot(left, right, left_dim, right_dim):
@@ -338,41 +533,16 @@
     send_w = jnp.pad(
         jnp.concatenate(slot_weights, axis=1), ((0, 0), (0, 8 - TOP), (0, -slots % 128))
     )
-    got_m, got_c, got_w = dispatch(send_m, send_c, send_w)
-    inputs = got_m.reshape(experts * slots, D)
-    side = lax.axis_index("sp") % TOP
-    weight = lax.dynamic_index_in_dim(got_w, side, 1, keepdims=False)[:, :slots]
-    seeds = (
-        (weight[:, :, None] * got_c.astype(jnp.float32))
-        .astype(jnp.bfloat16)
-        .reshape(experts * slots, D)
-    )
-    gate_mat = gate_w[0]
-    up_mat = up_w[0]
-    down_mat = down_w[0]
-    gate_pre = dot(inputs, gate_mat, 1, 0)
-    up_pre = dot(inputs, up_mat, 1, 0)
-    gate_act = jax.nn.silu(gate_pre)
-    hidden = (gate_act * up_pre).astype(jnp.bfloat16)
-    hidden_grad = dot(seeds, down_mat, 1, 1)
-    gate_grad = (hidden_grad * up_pre * silu_slope(gate_pre)).astype(jnp.bfloat16)
-    up_grad = (hidden_grad * gate_act).astype(jnp.bfloat16)
-    partial_value = (dot(gate_grad, gate_mat, 1, 1) + dot(up_grad, up_mat, 1, 1)).astype(
-        jnp.bfloat16
-    )
-    summed = lax.psum_scatter(partial_value, "tp", scatter_dimension=1, tiled=True)
-    returned = lax.all_to_all(
-        summed.reshape(experts, slots, width), "sp", split_axis=0, concat_axis=0, tiled=True
-    )
-    pick_each = jnp.repeat(pick.reshape(GROUPS, 1, slots, token_count), TOP, axis=1)
-    moe_grad = dot(
-        pick_each.reshape(experts * slots, token_count),
-        returned.reshape(experts * slots, width),
-        0,
-        0,
-    )
-    mid_part = (own_cot.astype(jnp.float32) + moe_grad).astype(jnp.bfloat16)
-    mid_grad = lax.all_gather(mid_part, "tp", axis=1, tiled=True)
+    own_slot = slot[None, :, None] == (
+        slots * jnp.arange(GROUPS, dtype=jnp.int32)[:, None, None]
+        + jnp.arange(slots, dtype=jnp.int32)[None, None, :]
+    )
+    mid_grad, inputs, seeds, hidden, gate_grad, up_grad = exchange(
+        send_m, send_c, send_w, own_slot.astype(jnp.bfloat16), own_cot, gate_w[0], up_w[0], down_w[0]
+    )
+    inputs, seeds, hidden, gate_grad, up_grad = (
+        each.reshape(experts * slots, -1) for each in (inputs, seeds, hidden, gate_grad, up_grad)
+    )
     grad_down = dot(hidden, seeds, 0, 0).astype(jnp.bfloat16)
     grad_gate = dot(inputs, gate_grad, 0, 0).astype(jnp.bfloat16)
     grad_up = dot(inputs, up_grad, 0, 0).astype(jnp.bfloat16)
@@ -389,12 +559,9 @@
             + conv_taps[lag_index].astype(jnp.float32)[None, :]
             * extended[lag_index : lag_index + token_count]
         )
-    grad_proj = lax.psum_scatter(
-        dot(mid_grad, activated, 0, 0).astype(jnp.bfloat16),
-        "sp",
-        scatter_dimension=0,
-        tiled=True,
-    ).astype(jnp.float32)
+    grad_proj = reduce_rows(
+        dot(mid_grad, activated, 0, 0).astype(jnp.bfloat16).reshape(experts, D // experts, -1)
+    )
     return (grad_gate[None], grad_up[None], grad_down[None], grad_proj, conv_input_grad)
 
 

time: 206 us -> 110 us (0.53)
  waiting for transfers between devices: 108 us -> 0.01 us
  Pallas kernels: 35.1 us -> 86.5 us
  matrix products: 32 us -> 13.9 us
  between operations: 14 us -> 0.85 us
  starting transfers between devices: 7.1 us -> 1.74 us
  other arithmetic: 5.7 us -> 3.2 us
    reduce_scatter x2 -> x0, waiting for transfers between devices: 78.3 us -> none  [the longest x1 49 us: paired_body(): lax.psum_scatter(dot(mid_grad, activated, 0, 0).astype(jnp.bfloat16), 'sp...]
    pallas_call x1 -> x2, Pallas kernels: 35.1 us -> 86.5 us  [the longest x1 62.7 us: exchange(): pl.pallas_call(exchange_kernel, out_shape=(jax.ShapeDtypeStruct((token_co...]
    dot_general x14 -> x8, matrix products: 32 us -> 13.9 us  [dot(): lax.dot_general(left, right, (((left_dim,), (right_dim,)), ((), ())), pre...]
    all_to_all x1 -> x0, waiting for transfers between devices: 15.6 us -> none  [paired_body(): lax.all_to_all(summed.reshape(experts, slots, width), 'sp', split_axis=0,...]
    all_gather x1 -> x0, waiting for transfers between devices: 9.91 us -> none  [paired_body(): mid_grad = lax.all_gather(mid_part, 'tp', axis=1, tiled=True)]
    all_to_all x1 -> x0, starting transfers between devices: 5.51 us -> none  [paired_body(): lax.all_to_all(summed.reshape(experts, slots, width), 'sp', split_axis=0,...]
    ppermute x1, waiting for transfers between devices: 4.31 us -> 0.01 us  [passed_along(): lax.ppermute(value, axis, [(source, source + steps) for source in range(i...]
    convert_element_type x3 -> x1, other arithmetic: 3.99 us -> 0.82 us  [paired_body(): own_slot.astype(jnp.bfloat16)]
  transfers between devices with their start and end apart: 5 -> 1, of which waited for: 5 -> 0; matrix products, arithmetic and copies ran while one was open for 7% -> 9% of each run, Pallas kernels for 0% -> 22%
where the time goes in v2:
time: 110 us
  Pallas kernels  86.5 us (79%)
  matrix products  13.9 us (13%)
  local copies, waits for them, and re-layouts  3.43 us (3%)
  other arithmetic  3.2 us (3%)
  starting transfers between devices  1.74 us (2%)
    pallas_call x1, Pallas kernels, exchange(): pl.pallas_call(exchange_kernel, out_shape=(jax.ShapeDtypeStruct((token_co...  62.7 us
    pallas_call x1, Pallas kernels, reduce_rows(): pl.pallas_call(reduce_kernel, out_shape=jax.ShapeDtypeStruct((rows, width...  23.8 us
    dot_general x8, matrix products, dot(): lax.dot_general(left, right, (((left_dim,), (right_dim,)), ((), ())), pre...  13.9 us
  transfers between devices with their start and end apart: 1, of which 0 were waited for; matrix products, arithmetic and copies ran while one was open for 9% of the time, Pallas kernels for 22%

profile of v2, /device:TPU:0, one launch (start us, length us, event | category | flops | bytes accessed | tf_op | source)
XLA Modules:
  0.0 109.6 jit_solution(5801865278484029296)
XLA Ops:
  0.6 0.0 copy-start
  0.7 0.8 slice.201
  1.4 0.2 fusion.4
  1.6 0.8 fusion.52
  2.4 0.2 select_reduce_fusion.1
  2.6 0.1 reshape.185
  2.7 0.1 reshape.186
  2.8 1.0 constant_dynamic-slice_fusion.cot
  3.7 0.0 copy-start.1
  3.8 1.0 convolution_convert_fusion.1
  4.7 0.0 copy-done
  4.7 1.0 convolution_convert_fusion.2
  5.7 0.1 iota_add_fusion
  5.8 0.8 compare_convert_fusion.pick
  6.6 0.6 select_maximum_fusion.send_w
  7.2 0.0 copy-done.1
  7.2 0.0 copy-start.5
  7.2 0.0 copy-start.10
  7.2 62.7 %exchange.1 = (bf16[256,2048]{1,0:T(8,128)(2,1)}, bf16[8,72,2048]{2,1,0:T(8,128)(2,1)}, bf16[8,72,2048]{2,1,0:T(8,128)(2,1)}, bf16[8,72,512]{2,1,0:T(8,128)(2,1)...) custom-call(bf16[4,72,512]{2,1,0:T(8,128)(2,1)} %bitcast.72, bf16[4,72,512]{2,1,0:T(8,128)(2,1)} %bitcast.73, ...), custom_call_target="tpu_custom_call" | custom-call | tf_op jit(solution)/shard_map/exchange/pallas_call | solution.py:387
  69.9 0.0 copy-start.6
  69.9 0.0 copy-done.5
  69.9 0.0 copy-done.10
  69.9 1.8 %fusion.3 = bf16[256,256]{1,0:T(8,128)(2,1)S(1)} fusion(bf16[256,2048]{1,0:T(8,128)(2,1)} %get-tuple-element.16, bf16[256,2048]{1,0:T(8,128)(2,1)S(1)} %copy-done.5, bf16[256,256]{1,0:T(8,128)(2,1)S(1)} %copy-done.10), kind=kOutput, calls=%fused_computation.10 | convolution fusion | flops 269090816 | bytes 2359296 | tf_op jit(solution)/shard_map/dot_general | solution.py:488
  71.7 0.0 copy-start.2
  71.7 0.0 copy-start.4
  71.7 0.0 copy-start.9
  71.7 1.7 %collective-permute-start = (bf16[30,256]{1,0:T(8,128)(2,1)S(1)}, bf16[30,256]{1,0:T(8,128)(2,1)S(1)}, u32[]{:S(2)}, u32[]{:S(2)}) collective-permute-start(bf16[30,256]{1,0:T(8,128)(2,1)S(1)} %slice.267), channel_id=1, source_target_pairs={{4,0},{8,4},{12,8},{16,12},{20,16},{24,20},{28,24},{5,1},{9,5},{13... | collective-permute-start | bytes 46088 | tf_op jit(solution)/shard_map/ppermute | solution.py:18
  73.5 0.0 copy-done.6
  73.5 0.5 convolution_convert_fusion
  74.0 0.0 copy-done.2
  74.0 0.0 copy-done.4
  74.0 0.0 copy-done.9
  74.1 0.0 copy-start.8
  74.1 3.2 %fusion.1 = bf16[1,2048,512]{2,1,0:T(8,128)(2,1)} fusion(bf16[8,72,2048]{2,1,0:T(8,128)(2,1)S(1)} %copy-done.4, bf16[8,72,512]{2,1,0:T(8,128)(2,1)S(1)} %copy-done.9), kind=kOutput, calls=%fused_computation.4 | convolution fusion | flops 1209008128 | bytes 5046272 | tf_op jit(solution)/shard_map/dot_general | solution.py:488
  77.3 0.0 copy-done.8
  77.3 0.0 copy-start.3
  77.3 0.0 copy-start.7
  77.3 3.2 %fusion = bf16[1,2048,512]{2,1,0:T(8,128)(2,1)} fusion(bf16[8,72,2048]{2,1,0:T(8,128)(2,1)S(1)} %copy-done.4, bf16[8,72,512]{2,1,0:T(8,128)(2,1)S(1)} %copy-done.8), kind=kOutput, calls=%fused_computation.3 | convolution fusion | flops 1209008128 | bytes 5046272 | tf_op jit(solution)/shard_map/dot_general | solution.py:488
  80.4 0.0 copy-done.3
  80.4 0.0 copy-done.7
  80.4 3.2 %fusion.2 = bf16[1,512,2048]{2,1,0:T(8,128)(2,1)} fusion(bf16[8,72,512]{2,1,0:T(8,128)(2,1)S(1)} %copy-done.7, bf16[8,72,2048]{2,1,0:T(8,128)(2,1)S(1)} %copy-done.3), kind=kOutput, calls=%fused_computation.5 | convolution fusion | flops 1209008128 | bytes 5046272 | tf_op jit(solution)/shard_map/dot_general | solution.py:488
  83.6 23.8 %reduce_rows.1 = f32[256,256]{1,0:T(8,128)S(1)} custom-call(bf16[8,256,256]{2,1,0:T(8,128)(2,1)S(1)} %bitcast.68), custom_call_target="tpu_custom_call" | custom-call | tf_op jit(solution)/shard_map/reduce_rows/pallas_call | solution.py:468
  107.4 0.0 collective-permute-done
  107.5 1.4 %fusion.11 = f32[256,256]{1,0:T(8,128)} fusion(f32[286,256]{1,0:T(8,128)S(1)} %maximum_convert_fusion, f32[256]{0:T(256)S(1)} %bitcast.108, f32[256]{0:T(256)S(1)} %bitcast.109, f32[256]{0:T(256)S(1)} %bitcast.80, f32[256]{0:T(256)S(1)} %bitcast.81, f32[256]{0:T(256)S(1)} %bitcast.82, f32[256]{0:T(256)S(1)} %bitcast.83, f32[256]{0:T(256)S(1)} %bitcast.84, ...), kind=kLoop, calls=%fused_computation.27 | loop fusion | flops 3997696 | bytes 8420352 | tf_op jit(solution)/shard_map/add | solution.py:558
  108.9 0.7 copy.16
  (8 shorter events, 0.1 us)
Async XLA Ops:
  0.6 4.1 %copy-start = (bf16[256,2048]{1,0:T(8,128)(2,1)S(1)}, bf16[256,2048]{1,0:T(8,128)(2,1)}, u32[]{:S(2)}) copy-start(bf16[256,2048]{1,0:T(8,128)(2,1)} %param.10) | copy-start | bytes 3145732
  3.7 3.5 %copy-start.1 = (bf16[256,512]{1,0:T(8,128)(2,1)}, bf16[256,512]{1,0:T(8,128)(2,1)S(1)}, u32[]{:S(2)}) copy-start(bf16[256,512]{1,0:T(8,128)(2,1)S(1)} %constant_dynamic-slice_fusion.cot) | copy-start | bytes 786436
  7.2 62.7 %copy-start.5 = (bf16[256,2048]{1,0:T(8,128)(2,1)S(1)}, bf16[256,2048]{1,0:T(8,128)(2,1)}, u32[]{:S(2)}) copy-start(bf16[256,2048]{1,0:T(8,128)(2,1)} %param.13) | copy-start | bytes 3145732
  7.2 62.7 %copy-start.10 = (bf16[256,256]{1,0:T(8,128)(2,1)S(1)}, bf16[256,256]{1,0:T(8,128)(2,1)}, u32[]{:S(2)}) copy-start(bf16[256,256]{1,0:T(8,128)(2,1)} %param.11) | copy-start | bytes 393220
  69.9 3.6 %copy-start.6 = (bf16[256,2048]{1,0:T(8,128)(2,1)S(1)}, bf16[256,2048]{1,0:T(8,128)(2,1)}, u32[]{:S(2)}) copy-start(bf16[256,2048]{1,0:T(8,128)(2,1)} %get-tuple-element.16) | copy-start | bytes 3145732
  71.7 2.3 %copy-start.2 = (bf16[31,256]{1,0:T(8,128)(2,1)S(1)}, bf16[31,256]{1,0:T(8,128)(2,1)}, u32[]{:S(2)}) copy-start(bf16[31,256]{1,0:T(8,128)(2,1)} %param.12) | copy-start | bytes 47620
  71.7 2.3 %copy-start.4 = (bf16[8,72,2048]{2,1,0:T(8,128)(2,1)S(1)}, bf16[8,72,2048]{2,1,0:T(8,128)(2,1)}, u32[]{:S(2)}) copy-start(bf16[8,72,2048]{2,1,0:T(8,128)(2,1)} %get-tuple-element.11) | copy-start | bytes 7077892
  71.7 2.3 %copy-start.9 = (bf16[8,72,512]{2,1,0:T(8,128)(2,1)S(1)}, bf16[8,72,512]{2,1,0:T(8,128)(2,1)}, u32[]{:S(2)}) copy-start(bf16[8,72,512]{2,1,0:T(8,128)(2,1)} %get-tuple-element.13) | copy-start | bytes 1769476
  71.7 35.7 %collective-permute-start = (bf16[30,256]{1,0:T(8,128)(2,1)S(1)}, bf16[30,256]{1,0:T(8,128)(2,1)S(1)}, u32[]{:S(2)}, u32[]{:S(2)}) collective-permute-start(bf16[30,256]{1,0:T(8,128)(2,1)S(1)} %slice.267), channel_id=1, source_target_pairs={{4,0},{8,4},{12,8},{16,12},{20,16},{24,20},{28,24},{5,1},{9,5},{13... | collective-permute-start | bytes 46088 | tf_op jit(solution)/shard_map/ppermute | solution.py:18
  74.1 3.2 %copy-start.8 = (bf16[8,72,512]{2,1,0:T(8,128)(2,1)S(1)}, bf16[8,72,512]{2,1,0:T(8,128)(2,1)}, u32[]{:S(2)}) copy-start(bf16[8,72,512]{2,1,0:T(8,128)(2,1)} %get-tuple-element.12) | copy-start | bytes 1769476
  77.3 3.2 %copy-start.3 = (bf16[8,72,2048]{2,1,0:T(8,128)(2,1)S(1)}, bf16[8,72,2048]{2,1,0:T(8,128)(2,1)}, u32[]{:S(2)}) copy-start(bf16[8,72,2048]{2,1,0:T(8,128)(2,1)} %get-tuple-element.15) | copy-start | bytes 7077892
  77.3 3.2 %copy-start.7 = (bf16[8,72,512]{2,1,0:T(8,128)(2,1)S(1)}, bf16[8,72,512]{2,1,0:T(8,128)(2,1)}, u32[]{:S(2)}) copy-start(bf16[8,72,512]{2,1,0:T(8,128)(2,1)} %get-tuple-element.14) | copy-start | bytes 1769476

commit v3 on v2

--- a/solution.py
+++ b/solution.py
@@ -423,65 +423,58 @@
     )(send_m, send_c, send_w, pick, cot, gate_mat, up_mat, down_mat)
 
 
-def reduce_kernel(prod, out, in_x, side_sum, in_z, s_sem, r_sem):
-    planes = in_x.shape[0]
-    plane, side, row, core, across, _, _ = neighbours()
+def reduce_kernel(kept, crossed, out, side_sum, in_z, s_sem, r_sem):
+    planes = kept.shape[0]
+    plane, side, row, core, _, _, _ = neighbours()
     tp = 2 * row + core
     to = [(TOP * ((plane + k + 1) % planes) + side, tp) for k in range(planes - 1)]
-    greet([across] + to)
-
-    def remote(source, target_ref, kind, k, device):
+    greet(to)
+
+    def remote(source, target_ref, k, device):
         copy = pltpu.make_async_remote_copy(
             src_ref=source,
             dst_ref=target_ref,
-            send_sem=s_sem.at[kind, k],
-            recv_sem=r_sem.at[kind, k],
+            send_sem=s_sem.at[k],
+            recv_sem=r_sem.at[k],
             device_id=device,
             device_id_type=MESH,
         )
         copy.start()
         return copy
 
-    rows_of = [TOP * ((plane + k + 1) % planes) for k in range(planes)]
-    crossing = [
-        remote(prod.at[rows_of[k] + 1 - side], in_x.at[k], 0, k, across) for k in range(planes)
-    ]
     climbing = []
-    for k in range(planes):
-        crossing[k].wait_recv()
-        both = wide(prod[rows_of[k] + side]) + wide(in_x[k])
-        if k < planes - 1:
-            side_sum[k] = both.astype(prod.dtype)
-            climbing.append(remote(side_sum.at[k], in_z.at[k], 1, k, to[k]))
+    for k in range(planes - 1):
+        at = (plane + k + 1) % planes
+        side_sum[k] = (wide(kept[at]) + wide(crossed[at])).astype(kept.dtype)
+        climbing.append(remote(side_sum.at[k], in_z.at[k], k, to[k]))
+    both = wide(kept[plane]) + wide(crossed[plane])
     for k in range(planes - 1):
         climbing[k].wait_recv()
         both += wide(in_z[k])
     out[...] = both
-    for copy in crossing + climbing:
+    for copy in climbing:
         copy.wait_send()
 
 
-def reduce_rows(prod):
-    blocks, rows, width = prod.shape
-    planes = blocks // TOP
+def reduce_rows(kept, crossed):
+    planes, rows, width = kept.shape
     vmem = pl.BlockSpec(memory_space=pltpu.VMEM)
     return pl.pallas_call(
         reduce_kernel,
         out_shape=jax.ShapeDtypeStruct((rows, width), jnp.float32),
-        in_specs=[vmem],
+        in_specs=[vmem, vmem],
         out_specs=vmem,
         scratch_shapes=[
-            pltpu.VMEM((planes, rows, width), prod.dtype),
-            pltpu.VMEM((planes - 1, rows, width), prod.dtype),
-            pltpu.VMEM((planes - 1, rows, width), prod.dtype),
-            pltpu.SemaphoreType.DMA((2, planes)),
-            pltpu.SemaphoreType.DMA((2, planes)),
+            pltpu.VMEM((planes - 1, rows, width), kept.dtype),
+            pltpu.VMEM((planes - 1, rows, width), kept.dtype),
+            pltpu.SemaphoreType.DMA((planes,)),
+            pltpu.SemaphoreType.DMA((planes,)),
         ],
         compiler_params=pltpu.CompilerParams(
             collective_id=2, has_side_effects=True, vmem_limit_bytes=32 * 1024 * 1024
         ),
         name="reduce_rows",
-    )(prod)
+    )(kept, crossed)
 
 
 def dot(left, right, left_dim, right_dim):
@@ -559,9 +552,13 @@
             + conv_taps[lag_index].astype(jnp.float32)[None, :]
             * extended[lag_index : lag_index + token_count]
         )
-    grad_proj = reduce_rows(
-        dot(mid_grad, activated, 0, 0).astype(jnp.bfloat16).reshape(experts, D // experts, -1)
-    )
+    prod = dot(mid_grad, activated, 0, 0).astype(jnp.bfloat16)
+    prod = prod.reshape(experts // TOP, TOP, D // experts, -1)
+    side = lax.axis_index("sp") % TOP
+    kept = lax.dynamic_index_in_dim(prod, side, 1, keepdims=False)
+    crossing = lax.dynamic_index_in_dim(prod, 1 - side, 1, keepdims=False)
+    crossed = lax.ppermute(crossing, "sp", [(i, i + 1 - 2 * (i % TOP)) for i in range(experts)])
+    grad_proj = reduce_rows(kept, crossed)
     return (grad_gate[None], grad_up[None], grad_down[None], grad_proj, conv_input_grad)
 
 

time: 110 us -> 106 us (0.964)
  Pallas kernels: 86.5 us -> 77.5 us
  starting transfers between devices: 1.74 us -> 4.19 us
  matrix products: 13.9 us -> 15.8 us
    pallas_call x1, Pallas kernels: 23.8 us -> 14.9 us  [reduce_rows(): pl.pallas_call(reduce_kernel, out_shape=jax.ShapeDtypeStruct((rows, width...]
    ppermute x0 -> x1, starting transfers between devices: none -> 2.71 us  [paired_body(): lax.ppermute(crossing, 'sp', [(i, i + 1 - 2 * (i % TOP)) for i in range(e...]
    dot_general x8, matrix products: 13.9 us -> 15.8 us  [dot(): lax.dot_general(left, right, (((left_dim,), (right_dim,)), ((), ())), pre...]
  transfers between devices with their start and end apart: 1 -> 2, of which waited for: 0 -> 0; matrix products, arithmetic and copies ran while one was open for 9% -> 13% of each run, Pallas kernels for 22% -> 0%
where the time goes in v3:
time: 106 us; the launch traced here: 105 us
  Pallas kernels  77.5 us (73%)
  matrix products  15.8 us (15%)
  starting transfers between devices  4.19 us (4%)
  local copies, waits for them, and re-layouts  3.5 us (3%)
  other arithmetic  3.2 us (3%)
    pallas_call x1, Pallas kernels, exchange(): pl.pallas_call(exchange_kernel, out_shape=(jax.ShapeDtypeStruct((token_co...  62.6 us
    dot_general x8, matrix products, dot(): lax.dot_general(left, right, (((left_dim,), (right_dim,)), ((), ())), pre...  15.8 us
    pallas_call x1, Pallas kernels, reduce_rows(): pl.pallas_call(reduce_kernel, out_shape=jax.ShapeDtypeStruct((rows, width...  14.9 us
    ppermute x1, starting transfers between devices, paired_body(): lax.ppermute(crossing, 'sp', [(i, i + 1 - 2 * (i % TOP)) for i in range(e...  2.71 us
  transfers between devices with their start and end apart: 2, of which 0 were waited for; matrix products, arithmetic and copies ran while one was open for 13% of the time, Pallas kernels for 0%

profile of v3, /device:TPU:0, one launch (start us, length us, event | category | flops | bytes accessed | tf_op | source)
XLA Modules:
  0.0 105.1 jit_solution(9531033635224328208)
XLA Ops:
  0.6 0.0 copy-start
  0.7 0.8 slice.201
  1.4 0.2 fusion.4
  1.6 0.8 fusion.52
  2.4 0.2 select_reduce_fusion.1
  2.6 0.1 reshape.185
  2.7 0.1 reshape.186
  2.8 1.0 constant_dynamic-slice_fusion.cot
  3.7 0.0 copy-start.1
  3.8 1.0 convolution_convert_fusion.1
  4.7 0.0 copy-done
  4.7 1.0 convolution_convert_fusion.2
  5.7 0.1 iota_add_fusion
  5.8 0.8 compare_convert_fusion.pick
  6.6 0.6 select_maximum_fusion.send_w
  7.2 0.0 copy-done.1
  7.2 0.0 copy-start.5
  7.2 0.0 copy-start.9
  7.2 62.6 %exchange.1 = (bf16[256,2048]{1,0:T(8,128)(2,1)}, bf16[8,72,2048]{2,1,0:T(8,128)(2,1)}, bf16[8,72,2048]{2,1,0:T(8,128)(2,1)}, bf16[8,72,512]{2,1,0:T(8,128)(2,1)...) custom-call(bf16[4,72,512]{2,1,0:T(8,128)(2,1)} %bitcast.79, bf16[4,72,512]{2,1,0:T(8,128)(2,1)} %bitcast.80, ...), custom_call_target="tpu_custom_call" | custom-call | tf_op jit(solution)/shard_map/exchange/pallas_call | solution.py:387
  69.9 0.0 copy-start.6
  69.9 0.0 copy-done.5
  69.9 0.0 copy-done.9
  69.9 1.8 %fusion.3 = bf16[256,256]{1,0:T(8,128)(2,1)S(1)} fusion(bf16[256,2048]{1,0:T(8,128)(2,1)} %get-tuple-element.16, bf16[256,2048]{1,0:T(8,128)(2,1)S(1)} %copy-done.5, bf16[256,256]{1,0:T(8,128)(2,1)S(1)} %copy-done.9), kind=kOutput, calls=%fused_computation.10 | convolution fusion | flops 269090816 | bytes 2359296 | tf_op jit(solution)/shard_map/dot_general | solution.py:481
  71.7 1.5 %collective-permute-start.1 = (bf16[30,256]{1,0:T(8,128)(2,1)S(1)}, bf16[30,256]{1,0:T(8,128)(2,1)S(1)}, u32[]{:S(2)}, u32[]{:S(2)}) collective-permute-start(bf16[30,256]{1,0:T(8,128)(2,1)S(1)} %slice.267), channel_id=1, source_target_pairs={{4,0},{8,4},{12,8},{16,12},{20,16},{24,20},{28,24},{5,1},{9,5},{13... | collective-permute-start | bytes 46088 | tf_op jit(solution)/shard_map/ppermute | solution.py:18
  73.2 0.0 copy-done.6
  73.2 0.0 copy-start.2
  73.2 0.5 convolution_convert_fusion
  73.7 0.1 dynamic-slice_bitcast_fusion
  73.8 2.7 %collective-permute-start = (bf16[4,256,256]{2,1,0:T(8,128)(2,1)S(1)}, bf16[4,256,256]{2,1,0:T(8,128)(2,1)S(1)}, u32[]{:S(2)}, u32[]{:S(2)}) collective-permute-start(bf16[4,256,256]{2,1,0:T(8,128)(2,1)S(1)} %get-tuple-element.19), channel_id=1, source_target_pairs={{0,4},{4,0},{8,12},{12,8},{16,20},{20,16},{24,28},{28,24},{1,5},{5... | collective-permute-start | bytes 1572872 | tf_op jit(solution)/shard_map/ppermute | solution.py:560
  76.5 0.0 copy-done.2
  76.6 0.0 copy-start.4
  76.6 0.0 copy-start.8
  76.6 5.1 %fusion.1 = bf16[1,2048,512]{2,1,0:T(8,128)(2,1)} fusion(bf16[8,72,2048]{2,1,0:T(8,128)(2,1)} %get-tuple-element.11, bf16[8,72,512]{2,1,0:T(8,128)(2,1)} %get-tuple-element.13), kind=kOutput, calls=%fused_computation.4 | convolution fusion | flops 1209008128 | bytes 5046272 | tf_op jit(solution)/shard_map/dot_general | solution.py:481
  81.7 0.0 copy-done.4
  81.7 0.0 copy-done.8
  81.7 0.0 copy-start.3
  81.7 0.0 copy-start.7
  81.7 3.2 %fusion = bf16[1,2048,512]{2,1,0:T(8,128)(2,1)} fusion(bf16[8,72,2048]{2,1,0:T(8,128)(2,1)S(1)} %copy-done.4, bf16[8,72,512]{2,1,0:T(8,128)(2,1)S(1)} %copy-done.8), kind=kOutput, calls=%fused_computation.3 | convolution fusion | flops 1209008128 | bytes 5046272 | tf_op jit(solution)/shard_map/dot_general | solution.py:481
  84.9 0.0 copy-done.3
  84.9 0.0 copy-done.7
  84.9 3.2 %fusion.2 = bf16[1,512,2048]{2,1,0:T(8,128)(2,1)} fusion(bf16[8,72,512]{2,1,0:T(8,128)(2,1)S(1)} %copy-done.7, bf16[8,72,2048]{2,1,0:T(8,128)(2,1)S(1)} %copy-done.3), kind=kOutput, calls=%fused_computation.5 | convolution fusion | flops 1209008128 | bytes 5046272 | tf_op jit(solution)/shard_map/dot_general | solution.py:481
  88.1 0.0 collective-permute-done.1
  88.1 1.4 %fusion.11 = f32[256,256]{1,0:T(8,128)} fusion(f32[286,256]{1,0:T(8,128)S(1)} %maximum_convert_fusion, f32[256]{0:T(256)S(1)} %bitcast.116, f32[256]{0:T(256)S(1)} %bitcast.117, f32[256]{0:T(256)S(1)} %bitcast.88, f32[256]{0:T(256)S(1)} %bitcast.89, f32[256]{0:T(256)S(1)} %bitcast.90, f32[256]{0:T(256)S(1)} %bitcast.91, f32[256]{0:T(256)S(1)} %bitcast.92, ...), kind=kLoop, calls=%fused_computation.29 | loop fusion | flops 3997696 | bytes 8420352 | tf_op jit(solution)/shard_map/add | solution.py:551
  89.5 0.0 collective-permute-done.crossed
  89.5 14.9 %reduce_rows.1 = f32[256,256]{1,0:T(8,128)S(1)} custom-call(bf16[4,256,256]{2,1,0:T(8,128)(2,1)S(1)} %get-tuple-element.20.kept, bf16[4,256,256]{2,1,0:T(8,128)(2,1)S(1)} %collective-permute-done.crossed), custom_call_target="tpu_custom_call" | custom-call | tf_op jit(solution)/shard_map/reduce_rows/pallas_call | solution.py:462
  104.4 0.7 copy.22
  (8 shorter events, 0.1 us)
Async XLA Ops:
  0.6 4.1 %copy-start = (bf16[256,2048]{1,0:T(8,128)(2,1)S(1)}, bf16[256,2048]{1,0:T(8,128)(2,1)}, u32[]{:S(2)}) copy-start(bf16[256,2048]{1,0:T(8,128)(2,1)} %param.10) | copy-start | bytes 3145732
  3.7 3.5 %copy-start.1 = (bf16[256,512]{1,0:T(8,128)(2,1)}, bf16[256,512]{1,0:T(8,128)(2,1)S(1)}, u32[]{:S(2)}) copy-start(bf16[256,512]{1,0:T(8,128)(2,1)S(1)} %constant_dynamic-slice_fusion.cot) | copy-start | bytes 786436
  7.2 62.7 %copy-start.5 = (bf16[256,2048]{1,0:T(8,128)(2,1)S(1)}, bf16[256,2048]{1,0:T(8,128)(2,1)}, u32[]{:S(2)}) copy-start(bf16[256,2048]{1,0:T(8,128)(2,1)} %param.13) | copy-start | bytes 3145732
  7.2 62.7 %copy-start.9 = (bf16[256,256]{1,0:T(8,128)(2,1)S(1)}, bf16[256,256]{1,0:T(8,128)(2,1)}, u32[]{:S(2)}) copy-start(bf16[256,256]{1,0:T(8,128)(2,1)} %param.11) | copy-start | bytes 393220
  69.9 3.3 %copy-start.6 = (bf16[256,2048]{1,0:T(8,128)(2,1)S(1)}, bf16[256,2048]{1,0:T(8,128)(2,1)}, u32[]{:S(2)}) copy-start(bf16[256,2048]{1,0:T(8,128)(2,1)} %get-tuple-element.16) | copy-start | bytes 3145732
  71.7 16.4 %collective-permute-start.1 = (bf16[30,256]{1,0:T(8,128)(2,1)S(1)}, bf16[30,256]{1,0:T(8,128)(2,1)S(1)}, u32[]{:S(2)}, u32[]{:S(2)}) collective-permute-start(bf16[30,256]{1,0:T(8,128)(2,1)S(1)} %slice.267), channel_id=1, source_target_pairs={{4,0},{8,4},{12,8},{16,12},{20,16},{24,20},{28,24},{5,1},{9,5},{13... | collective-permute-start | bytes 46088 | tf_op jit(solution)/shard_map/ppermute | solution.py:18
  73.2 3.3 %copy-start.2 = (bf16[31,256]{1,0:T(8,128)(2,1)S(1)}, bf16[31,256]{1,0:T(8,128)(2,1)}, u32[]{:S(2)}) copy-start(bf16[31,256]{1,0:T(8,128)(2,1)} %param.12) | copy-start | bytes 47620
  73.8 15.7 %collective-permute-start = (bf16[4,256,256]{2,1,0:T(8,128)(2,1)S(1)}, bf16[4,256,256]{2,1,0:T(8,128)(2,1)S(1)}, u32[]{:S(2)}, u32[]{:S(2)}) collective-permute-start(bf16[4,256,256]{2,1,0:T(8,128)(2,1)S(1)} %get-tuple-element.19), channel_id=1, source_target_pairs={{0,4},{4,0},{8,12},{12,8},{16,20},{20,16},{24,28},{28,24},{1,5},{5... | collective-permute-start | bytes 1572872 | tf_op jit(solution)/shard_map/ppermute | solution.py:560
  76.6 5.1 %copy-start.4 = (bf16[8,72,2048]{2,1,0:T(8,128)(2,1)S(1)}, bf16[8,72,2048]{2,1,0:T(8,128)(2,1)}, u32[]{:S(2)}) copy-start(bf16[8,72,2048]{2,1,0:T(8,128)(2,1)} %get-tuple-element.11) | copy-start | bytes 7077892
  76.6 5.1 %copy-start.8 = (bf16[8,72,512]{2,1,0:T(8,128)(2,1)S(1)}, bf16[8,72,512]{2,1,0:T(8,128)(2,1)}, u32[]{:S(2)}) copy-start(bf16[8,72,512]{2,1,0:T(8,128)(2,1)} %get-tuple-element.12) | copy-start | bytes 1769476
  81.7 3.2 %copy-start.3 = (bf16[8,72,2048]{2,1,0:T(8,128)(2,1)S(1)}, bf16[8,72,2048]{2,1,0:T(8,128)(2,1)}, u32[]{:S(2)}) copy-start(bf16[8,72,2048]{2,1,0:T(8,128)(2,1)} %get-tuple-element.15) | copy-start | bytes 7077892
  81.7 3.2 %copy-start.7 = (bf16[8,72,512]{2,1,0:T(8,128)(2,1)S(1)}, bf16[8,72,512]{2,1,0:T(8,128)(2,1)}, u32[]{:S(2)}) copy-start(bf16[8,72,512]{2,1,0:T(8,128)(2,1)} %get-tuple-element.14) | copy-start | bytes 1769476
